TPU v7x, 128 devices: a whole 4x4x4 slice. The times are simulated.
128 devices in a mesh: sp: 16 (over z, x), dp: 8 (over y, core).
Axes of the slice: x: 4, y: 4, z: 4, core: 2. Of those that a mesh axis runs over, the one named last changes fastest.
Arguments:
- skip_stream_entering: bfloat16 [8, 2048, 2048], P('dp', 'sp'), may hold values from -6 to 6
- mapped_probe_matrix: bfloat16 [8, 2048, 2048], P('dp', 'sp'), may hold values from -6 to 6
- mapped_lookup_matrix: bfloat16 [8, 2048, 2048], P('dp', 'sp'), may hold values from -6 to 6
- mapped_content_matrix: bfloat16 [8, 2048, 4096], P('dp', 'sp'), may hold values from -6 to 6
- retention_preactivation: bfloat16 [8, 2048, 2048], P('dp', 'sp'), may hold values from -4 to 12
- extra_shrinkage: float32 [8, 16, 2048], P('dp', 'sp'), may hold values from -0.6932 to 0
- attention_group_scale: float32 [4096], replicated, may hold values from 0.1 to 1.9
- final_projection_matrix: bfloat16 [4096, 2048], P(None, 'dp'), may hold values from -0.09375 to 0.09375
- blender_branch_scale: float32 [2048], replicated, may hold values from 0.1 to 1.9
- specialist_prenormal_scale: float32 [2048], replicated, may hold values from 0.1 to 1.9
- specialist_switch_matrix: bfloat16 [128, 2048, 1024], P(('sp', 'dp')), may hold values from -0.125 to 0.125
- specialist_expand_matrix: bfloat16 [128, 2048, 1024], P(('sp', 'dp')), may hold values from -0.125 to 0.125
- specialist_contract_matrix: bfloat16 [128, 1024, 2048], P(('sp', 'dp')), may hold values from -0.1875 to 0.1875
- specialist_branch_scale: float32 [2048], replicated, may hold values from 0.1 to 1.9
- assigned_specialists: int32 [8, 2048, 2], P('dp', 'sp'), may hold values from 0 to 127, all different within a row; in each aligned block of 128 rows (0 to 127, 128 to 255, ..., all dimensions but the last counted through in order) at most 3 rows name the same one
- dispatcher_logits: float32 [8, 2048, 2], P('dp', 'sp'), may hold values from 0.2 to 1
Outputs:
- layer_out: bfloat16 [8, 2048, 2048], P('dp', 'sp')
Inputs may be any that keep to these rules, and one draw needn't show every extreme that they name: `assigned_specialists`: in the rows of one device no expert is named more than 3 times; in every draw some expert reaches 3 on some device.
All inputs are finite; a program needn't handle non-finite values.
Results may differ from a plain program's by a relative error of at most 0.013.
Values may be sent and summed in bfloat16 or wider, within the bound.
No kernel may reach another device: no remote copies, remote signals or barrier semaphores. Data moves between devices by JAX's collectives and lax.ppermute only.
A program may use at most 128 MiB of HBM per device.

v0:
```python
import jax
import jax.numpy as jnp
from jax import lax
from jax.sharding import PartitionSpec as P

D = 2048
ATTENTION_GROUPS = 16
KEY_WIDTH = 128
DV = 256
TOP = 2
BLOCK = 64


epsilon = 1e-06
softness_factor = 16.0


def sent_together(arrays, axis, split_dim, concat_dim, along):
    ends, at = ([], 0)
    for a in arrays[:-1]:
        at += a.shape[along]
        ends.append(at)
    both = jnp.concatenate(arrays, axis=along)
    return tuple(
        jnp.split(
            lax.all_to_all(both, axis, split_axis=split_dim, concat_axis=concat_dim, tiled=True),
            ends,
            axis=along,
        )
    )


def split_up(value, dim, size):
    before, after = (value.shape[:dim], value.shape[dim + 1 :])
    return jnp.moveaxis(value.reshape(*before, size, -1, *after), dim, 0)


def in_order(pieces, dim):
    shape = list(pieces.shape[1:])
    shape[dim] *= pieces.shape[0]
    return jnp.moveaxis(pieces, 0, dim).reshape(shape)


def one_exchange(value, axis, axes, splits, concats):
    sizes = [lax.axis_size(a) for a in axes]
    pieces = split_up(value, splits[0], sizes[0])
    pieces = jnp.moveaxis(split_up(pieces, splits[1] + 1, sizes[1]), 0, 1)
    inside = pieces.shape[2:]
    pieces = pieces.reshape(-1, *inside)
    pieces = lax.all_to_all(pieces, axis, split_axis=0, concat_axis=0, tiled=True)
    pieces = in_order(pieces.reshape(*sizes, *inside), concats[0] + 1)
    return in_order(pieces, concats[1])


def rms_scale(values, gain):
    mean_square = jnp.mean(values * values, axis=-1, keepdims=True)
    return values * lax.rsqrt(mean_square + epsilon) * gain


def combine_states(earlier, later):
    return (earlier[0] * later[0], later[0][..., None] * earlier[1] + later[1])


def block_attention(query_f, key_f, value_f, shrink_exponent):
    length_value, head_count, key_dim = query_f.shape
    value_dim = value_f.shape[-1]
    block_count = length_value // BLOCK
    query_blocks = query_f.reshape(block_count, BLOCK, head_count, key_dim)
    key_blocks = key_f.reshape(block_count, BLOCK, head_count, key_dim)
    value_blocks = value_f.reshape(block_count, BLOCK, head_count, value_dim)
    within = jnp.cumsum(shrink_exponent.reshape(block_count, BLOCK, head_count, key_dim), axis=1)
    block_end = within[:, -1]
    lifted = query_blocks * jnp.exp(within)
    lowered = key_blocks * jnp.exp(-within)
    scores = jnp.einsum("nthk,nshk->nhts", lifted, lowered)
    causal = jnp.arange(BLOCK)[:, None] >= jnp.arange(BLOCK)[None, :]
    scores = jnp.where(causal, scores, 0.0)
    inside = jnp.einsum("nhts,nshv->nthv", scores, value_blocks)
    carried_keys = key_blocks * jnp.exp(block_end[:, None] - within)
    updates = jnp.einsum("nshk,nshv->nhkv", carried_keys, value_blocks)
    decays = jnp.exp(block_end)
    total_decay, states = lax.associative_scan(combine_states, (decays, updates), axis=0)
    entering = jnp.concatenate([jnp.zeros_like(states[:1]), states[:-1]], axis=0)
    across = jnp.einsum("nthk,nhkv->nthv", lifted, entering)
    outputs = (inside + across).reshape(length_value, head_count, value_dim)
    offsets = jnp.cumsum(block_end, axis=0) - block_end
    reached = (query_blocks * jnp.exp(within + offsets[:, None])).reshape(
        length_value, head_count, key_dim
    )
    return (outputs, total_decay[-1], states[-1], reached)


def shards(
    skip_stream_entering,
    mapped_probe_matrix,
    mapped_lookup_matrix,
    mapped_content_matrix,
    retention_preactivation,
    extra_shrinkage,
    attention_group_scale,
    final_projection_matrix,
    blender_branch_scale,
    specialist_prenormal_scale,
    specialist_switch_matrix,
    specialist_expand_matrix,
    specialist_contract_matrix,
    specialist_branch_scale,
    assigned_specialists,
    dispatcher_logits,
):
    tok_rows = mapped_probe_matrix.shape[1]
    sp_count = lax.axis_size("sp")
    dp_count = lax.axis_size("dp")
    query_local = mapped_probe_matrix[0].reshape(tok_rows, ATTENTION_GROUPS, KEY_WIDTH)
    key_local = mapped_lookup_matrix[0].reshape(tok_rows, ATTENTION_GROUPS, KEY_WIDTH)
    value_local = mapped_content_matrix[0].reshape(tok_rows, ATTENTION_GROUPS, DV)
    decay_local = retention_preactivation[0].reshape(tok_rows, ATTENTION_GROUPS, KEY_WIDTH)
    arrived = sent_together((query_local, key_local, value_local, decay_local), "sp", 1, 0, 2)
    query_head, key_head, value_head, head_decay = arrived
    own_heads = query_head.shape[1]
    shrink_exponent = jax.nn.log_sigmoid(head_decay.astype(jnp.float32)) / softness_factor
    shrink_exponent = shrink_exponent + jnp.transpose(extra_shrinkage[0])[:, :, None]
    outputs = block_attention(
        query_head.astype(jnp.float32) * KEY_WIDTH ** (-0.5),
        key_head.astype(jnp.float32),
        value_head.astype(jnp.float32),
        shrink_exponent,
    )[0]
    offset = lax.axis_index("sp") * (own_heads * DV)
    gains = lax.dynamic_slice_in_dim(attention_group_scale, offset, own_heads * DV).reshape(
        own_heads, DV
    )
    normed = rms_scale(outputs, gains).astype(jnp.bfloat16)
    attention_group_result = lax.all_to_all(normed, "sp", split_axis=0, concat_axis=1, tiled=True)
    flat_heads = attention_group_result.reshape(tok_rows, ATTENTION_GROUPS * DV)
    projected = jnp.dot(
        flat_heads,
        lax.all_gather(final_projection_matrix, "dp", axis=1, tiled=True),
        preferred_element_type=jnp.float32,
    ).astype(jnp.bfloat16)
    stream = skip_stream_entering[0].astype(jnp.float32)
    residual = (stream + rms_scale(projected.astype(jnp.float32), blender_branch_scale)).astype(
        jnp.bfloat16
    )
    expert_in = rms_scale(residual.astype(jnp.float32), specialist_prenormal_scale).astype(
        jnp.bfloat16
    )
    expert_total = sp_count * dp_count
    capacity = max(2, 5 * tok_rows * TOP // (3 * expert_total))
    chosen = assigned_specialists[0].reshape(-1)
    pair_total = chosen.shape[0]
    onehot = (chosen[:, None] == jnp.arange(expert_total, dtype=jnp.int32)[None, :]).astype(
        jnp.int32
    )
    ranks = jnp.sum((jnp.cumsum(onehot, axis=0) - onehot) * onehot, axis=1)
    slots = chosen * capacity + ranks
    table = jnp.full((expert_total * capacity,), pair_total, jnp.int32)
    table = table.at[slots].set(jnp.arange(pair_total, dtype=jnp.int32))
    padded = jnp.concatenate([expert_in, jnp.zeros((1, D), jnp.bfloat16)], axis=0)
    outgoing = padded[table // TOP].reshape(expert_total, capacity, D)
    grid = outgoing.reshape(sp_count, dp_count, capacity, D)
    arrived_grid = one_exchange(grid, ("sp", "dp"), ("sp", "dp"), (0, 1), (0, 1))
    row_block = arrived_grid.reshape(-1, D)
    gate_part = jnp.dot(row_block, specialist_switch_matrix[0], preferred_element_type=jnp.float32)
    up_part = jnp.dot(row_block, specialist_expand_matrix[0], preferred_element_type=jnp.float32)
    hidden_units = (jax.nn.silu(gate_part) * up_part).astype(jnp.bfloat16)
    result = jnp.dot(
        hidden_units, specialist_contract_matrix[0], preferred_element_type=jnp.float32
    )
    processed = result.astype(jnp.bfloat16).reshape(arrived_grid.shape)
    returned = one_exchange(processed, ("sp", "dp"), ("sp", "dp"), (0, 1), (0, 1))
    flat_back = returned.reshape(expert_total * capacity, D)
    pair_rows = flat_back[slots].reshape(tok_rows, TOP, D)
    weights = dispatcher_logits[0]
    weights = weights / jnp.sum(weights, axis=1, keepdims=True)
    combined = jnp.sum(pair_rows.astype(jnp.float32) * weights[:, :, None], axis=1)
    layer_out = residual.astype(jnp.float32) + rms_scale(combined, specialist_branch_scale)
    return layer_out.astype(jnp.bfloat16)[None]


def solution(mesh):
    return jax.shard_map(
        shards,
        mesh=mesh,
        in_specs=(
            P("dp", "sp", None),
            P("dp", "sp", None),
            P("dp", "sp", None),
            P("dp", "sp", None),
            P("dp", "sp", None),
            P("dp", "sp", None),
            P(),
            P(None, "dp"),
            P(),
            P(),
            P(("sp", "dp"), None, None),
            P(("sp", "dp"), None, None),
            P(("sp", "dp"), None, None),
            P(),
            P("dp", "sp", None),
            P("dp", "sp", None),
        ),
        out_specs=P("dp", "sp", None),
        check_vma=False,
    )
```

profile of v0, /device:TPU:1, one launch (start us, length us, event | category | flops | bytes accessed | tf_op | source)
XLA Modules:
  0.0 298.4 jit_solution(1398296996152553619)
XLA Ops:
  11.8 8.5 %all-to-all-start = ((bf16[128,16,640]{2,0,1:T(8,128)(2,1)}), bf16[128,16,640]{2,0,1:T(8,128)(2,1)S(1)}, u32[]{:S(2)}, u32[]{:S(2)}) async-start(bf16[128,16,640]{2,0,1:T(8,128)(2,1)} %pad_maximum_fusion), calls=%async_computation | async-start | bytes 5242880 | tf_op jit(solution)/shard_map/all_to_all | solution.py:26
  21.8 37.6 %all-to-all-done = bf16[128,16,640]{2,0,1:T(8,128)(2,1)S(1)} async-done(((bf16[128,16,640]{2,0,1:T(8,128)(2,1)}), bf16[128,16,640]{2,0,1:T(8,128)(2,1)S(1)}, u32[]{:S(2)}, u32[]{:S(2)}) %all-to-all-start) | async-done | bytes 2621472 | tf_op jit(solution)/shard_map/all_to_all | solution.py:26
  79.6 4.2 %pad.38 = f32[8,1,128,256]{3,2,0,1:T(8,128)} pad(f32[4,1,128,256]{3,2,0,1:T(8,128)} %add.178, f32[]{:T(128)} %constant.27.clone.1), padding=1_0_1x0_0_0x0_0_0x0_0_0 | pad | bytes 1572868 | tf_op jit(solution)/shard_map/pad | solution.py:82
  86.0 4.1 %pad.37 = f32[8,1,128,256]{3,2,0,1:T(8,128)} pad(f32[4,1,128,256]{3,2,0,1:T(8,128)} %pad_maximum_fusion.3, f32[]{:T(128)} %constant.27.clone.1), padding=0_1_1x0_0_0x0_0_0x0_0_0 | pad | bytes 1572868 | tf_op jit(solution)/shard_map/pad | solution.py:82
  94.9 4.0 %pad.39 = f32[16,1,128,256]{3,2,0,1:T(8,128)S(1)} pad(f32[8,1,128,256]{3,2,0,1:T(8,128)} %pad_maximum_fusion.2, f32[]{:T(128)} %constant.27.clone.1), padding=0_1_1x0_0_0x0_0_0x0_0_0 | pad | bytes 3145732 | tf_op jit(solution)/shard_map/pad | solution.py:82
  98.9 6.5 %pad.40 = f32[16,1,128,256]{3,2,0,1:T(8,128)} pad(f32[8,1,128,256]{3,2,0,1:T(8,128)} %add.180, f32[]{:T(128)} %constant.27.clone.1), padding=1_0_1x0_0_0x0_0_0x0_0_0 | pad | bytes 3145732 | tf_op jit(solution)/shard_map/pad | solution.py:82
  105.4 3.2 %add.182 = f32[16,1,128,256]{3,2,0,1:T(8,128)} add(f32[16,1,128,256]{3,2,0,1:T(8,128)S(1)} %pad.39, f32[16,1,128,256]{3,2,0,1:T(8,128)} %pad.40) | non-fusion elementwise | flops 524288 | bytes 6291456 | tf_op jit(solution)/shard_map/add | solution.py:82
  108.6 11.4 %pad.86 = f32[32,1,128,256]{3,2,0,1:T(8,128)} pad(f32[16,1,128,256]{3,2,0,1:T(8,128)} %add.182, f32[]{:T(128)} %constant.27.clone.1), padding=1_0_1x0_0_0x0_0_0x0_0_0 | pad | bytes 6291460
  123.7 7.2 %pad.58 = f32[31,1,128,256]{3,2,0,1:T(8,128)} pad(f32[16,1,128,256]{3,2,0,1:T(8,128)S(1)} %pad_maximum_fusion.1, f32[]{:T(128)} %constant.27.clone.1), padding=0_0_1x0_0_0x0_0_0x0_0_0 | pad | bytes 6160388 | tf_op jit(solution)/shard_map/slice | solution.py:83
  132.9 4.1 %slice_add_fusion.5 = bf16[31,1,128,256]{3,2,0,1:T(8,128)(2,1)S(1)} fusion(f32[31,1,128,256]{3,2,0,1:T(8,128)} %pad.58, f32[32,1,128,256]{3,2,0,1:T(8,128)} %pad.86), kind=kLoop, calls=%fused_computation.121 | loop fusion | flops 2031616 | bytes 10158080 | tf_op jit(solution)/shard_map/add | solution.py:82
  144.0 3.7 %all-to-all-start.1 = ((bf16[16,2,16384]{2,1,0:T(2,128)(2,1)}), bf16[16,2,16384]{2,1,0:T(2,128)(2,1)S(1)}, u32[]{:S(2)}, u32[]{:S(2)}) async-start(bf16[16,2,16384]{2,1,0:T(2,128)(2,1)} %reshape.349), calls=%async_computation.1 | async-start | bytes 2097152 | tf_op jit(solution)/shard_map/all_to_all | solution.py:134
  149.9 12.8 %all-to-all-done.1 = bf16[16,2,16384]{2,1,0:T(2,128)(2,1)S(1)} async-done(((bf16[16,2,16384]{2,1,0:T(2,128)(2,1)}), bf16[16,2,16384]{2,1,0:T(2,128)(2,1)S(1)}, u32[]{:S(2)}, u32[]{:S(2)}) %all-to-all-start.1) | async-done | bytes 1048608 | tf_op jit(solution)/shard_map/all_to_all | solution.py:134
  164.7 8.3 %multiply_reduce_fusion.2 = (f32[128]{0:T(128)S(1)}, f32[128,2048]{1,0:T(8,128)S(1)}) fusion(bf16[128,4096]{0,1:T(8,128)(2,1)S(1)} %bitcast.154, bf16[4096,2048]{1,0:T(8,128)(2,1)} %all-gather.2.cloned.1.call-done), kind=kOutput, calls=%fused_computation.58 | convolution fusion | flops 2148532224 | bytes 18874880 | tf_op jit(solution)/shard_map/dot_general | solution.py:136
  173.9 3.1 %gather_fusion = bf16[384,2048]{1,0:T(8,128)(2,1)} fusion(bf16[129,2048]{1,0:T(8,128)(2,1)S(1)} %concatenate.27, s32[1024]{0:T(1024)S(1)} %pad_clamp_fusion.1), kind=kCustom, calls=%fused_computation | custom fusion | bytes 3147264 | tf_op jit(solution)/shard_map/gather | solution.py:160
  177.0 4.0 %reshape_transpose_transpose_reshape_reshape_reshape_reshape.3 = bf16[128,1,1,3,2048]{4,3,0,2,1:T(4,128)(2,1)S(1)} reshape(bf16[384,2048]{1,0:T(8,128)(2,1)} %gather_fusion) | data formatting | bytes 3145728 | tf_op jit(solution)/shard_map/reshape;transpose;transpose;reshape;reshape;reshape;reshape | solution.py:49
  181.0 38.3 %all_to_all.43 = bf16[128,1,1,3,2048]{4,3,2,1,0:T(4,128)(2,1)} all-to-all(bf16[128,1,1,3,2048]{4,3,2,1,0:T(4,128)(2,1)S(1)} %bitcast.152), channel_id=1, replica_groups=mesh['sp'=16,'dp'=8] {'sp','dp'}, dimensions={0} | all-to-all | bytes 3145728 | tf_op jit(solution)/shard_map/all_to_all | solution.py:50
  219.3 3.9 %reshape_reshape.6 = bf16[384,2048]{1,0:T(8,128)(2,1)S(1)} reshape(bf16[16,8,1,3,2048]{4,3,1,0,2:T(4,128)(2,1)} %bitcast.153) | data formatting | bytes 3145728 | tf_op jit(solution)/shard_map/reshape;reshape | solution.py:163
  223.2 5.1 %fusion.4 = f32[384,1024]{1,0:T(8,128)} fusion(bf16[384,2048]{1,0:T(8,128)(2,1)S(1)} %reshape_reshape.6, bf16[1,2048,1024]{2,1,0:T(8,128)(2,1)} %param.26), kind=kOutput, calls=%fused_computation.7 | convolution fusion | flops 1610612736 | bytes 7340032 | tf_op jit(solution)/shard_map/dot_general | solution.py:164
  228.3 8.6 %fusion.9 = bf16[384,2048]{1,0:T(8,128)(2,1)} fusion(bf16[1,1024,2048]{2,1,0:T(8,128)(2,1)} %param.28, f32[384,1024]{1,0:T(8,128)} %fusion.4, bf16[384,2048]{1,0:T(8,128)(2,1)S(1)} %reshape_reshape.6, bf16[1,2048,1024]{2,1,0:T(8,128)(2,1)} %param.27), kind=kOutput, calls=%fused_computation.13 | convolution fusion | flops 3224371200 | bytes 13107200 | tf_op jit(solution)/shard_map/dot_general | solution.py:167
  236.9 5.2 %reshape_transpose_transpose_reshape_reshape_reshape.3 = bf16[128,1,1,3,2048]{4,3,0,2,1:T(4,128)(2,1)} reshape(bf16[384,2048]{1,0:T(8,128)(2,1)} %fusion.9) | data formatting | bytes 3145728 | tf_op jit(solution)/shard_map/reshape;transpose;transpose;reshape;reshape;reshape | solution.py:49
  242.1 4.9 %all-to-all-start.3 = ((bf16[128,1,1,3,2048]{4,3,2,1,0:T(4,128)(2,1)}), bf16[128,1,1,3,2048]{4,3,2,1,0:T(4,128)(2,1)S(1)}, u32[]{:S(2)}, u32[]{:S(2)}) async-start(bf16[128,1,1,3,2048]{4,3,2,1,0:T(4,128)(2,1)} %bitcast.151), calls=%async_computation.3 | async-start | bytes 4194304 | tf_op jit(solution)/shard_map/all_to_all | solution.py:50
  247.1 30.1 %all-to-all-done.3 = bf16[128,1,1,3,2048]{4,3,2,1,0:T(4,128)(2,1)S(1)} async-done(((bf16[128,1,1,3,2048]{4,3,2,1,0:T(4,128)(2,1)}), bf16[128,1,1,3,2048]{4,3,2,1,0:T(4,128)(2,1)S(1)}, u32[]{:S(2)}, u32[]{:S(2)}) %all-to-all-start.3) | async-done | bytes 1572896 | tf_op jit(solution)/shard_map/all_to_all | solution.py:50
  278.5 3.9 %reshape_reshape.7 = bf16[384,2048]{1,0:T(8,128)(2,1)S(1)} reshape(bf16[16,8,1,3,2048]{4,3,1,0,2:T(4,128)(2,1)} %bitcast.150) | data formatting | bytes 3145728 | tf_op jit(solution)/shard_map/reshape;reshape | solution.py:172
  287.2 3.2 %multiply_reduce_fusion = f32[128,2048]{1,0:T(8,128)S(1)} fusion(f32[128,2,2048]{2,1,0:T(2,128)S(1)} %reshape.321, f32[128,2]{1,0:T(8,128)S(1)} %copy.99), kind=kLoop, calls=%fused_computation.23 | loop fusion | flops 786432 | bytes 3146752 | tf_op jit(solution)/shard_map/reduce_sum | solution.py:176
  (153 shorter events, 58.5 us)
Async XLA Ops:
  6.5 1.2 copy-start.8
  6.5 158.1 %all-gather.2.cloned.1.call-start = ((), (), s32[]{:S(2)}) async-start(), calls=%async_computation.4 | async-start | bytes 18874368 | tf_op jit(solution)/shard_map/all_gather | solution.py:138
  8.0 1.1 copy-start.13
  11.8 8.6 %copy-start.21 = (s32[1,128,2]{1,2,0:T(2,128)S(1)}, s32[1,128,2]{1,2,0:T(2,128)}, u32[]{:S(2)}) copy-start(s32[1,128,2]{1,2,0:T(2,128)} %param.30) | copy-start | bytes 3076
  11.8 47.6 %all-to-all-start = ((bf16[128,16,640]{2,0,1:T(8,128)(2,1)}), bf16[128,16,640]{2,0,1:T(8,128)(2,1)S(1)}, u32[]{:S(2)}, u32[]{:S(2)}) async-start(bf16[128,16,640]{2,0,1:T(8,128)(2,1)} %pad_maximum_fusion), calls=%async_computation | async-start | bytes 5242880 | tf_op jit(solution)/shard_map/all_to_all | solution.py:26
  20.4 40.2 %copy-start.16 = (f32[1,1,2048]{2,1,0:T(1,128)S(1)}, f32[1,1,2048]{2,1,0:T(1,128)}, u32[]{:S(2)}) copy-start(f32[1,1,2048]{2,1,0:T(1,128)} %param.21) | copy-start | bytes 24580
  21.0 38.5 %copy-start.9 = (s32[128,2,128]{0,1,2:T(2,128)}, s32[128,2,128]{0,1,2:T(2,128)S(1)}, u32[]{:S(2)}) copy-start(s32[128,2,128]{0,1,2:T(2,128)S(1)} %fusion.53) | copy-start | bytes 393220
  21.0 41.3 %copy-start.20 = (s32[128,3]{0,1:T(4,128)}, s32[128,3]{0,1:T(4,128)S(1)}, u32[]{:S(2)}) copy-start(s32[128,3]{0,1:T(4,128)S(1)} %reduce-window.9) | copy-start | bytes 4612
  62.3 1.2 copy-start.7
  63.5 2.5 copy-start.1
  66.8 1.9 copy-start
  77.5 7.7 %slice-start = ((f32[8,1,128,256]{3,2,0,1:T(8,128)}), f32[1,1,128,256]{3,2,0,1:T(8,128)S(1)}, s32[]{:S(2)}) async-start(f32[8,1,128,256]{3,2,0,1:T(8,128)} %copy-done.5), calls=%async_computation.5 | async-start | bytes 262144 | tf_op jit(solution)/shard_map/slice | solution.py:82
  90.1 2.8 copy-start.2
  90.1 2.8 copy-start.3
  132.9 4.1 %copy-start.6 = (bf16[32,64,128]{2,0,1:T(8,128)(2,1)S(1)}, bf16[32,64,128]{2,0,1:T(8,128)(2,1)}, u32[]{:S(2)}) copy-start(bf16[32,64,128]{2,0,1:T(8,128)(2,1)} %get-tuple-element.13) | copy-start | bytes 1572868
  142.8 4.8 %slice-start.1 = ((s32[128,3]{0,1:T(4,128)}), s32[128,2]{0,1:T(2,128)S(1)}, s32[]{:S(2)}) async-start(s32[128,3]{0,1:T(4,128)} %copy-done.20), calls=%async_computation.6 | async-start | bytes 2048 | tf_op jit(solution)/shard_map/slice.1
  142.8 4.8 %copy-start.10 = (s32[128,2,128]{0,1,2:T(2,128)S(1)}, s32[128,2,128]{0,1,2:T(2,128)}, u32[]{:S(2)}) copy-start(s32[128,2,128]{0,1,2:T(2,128)} %copy-done.9) | copy-start | bytes 393220
  144.0 18.7 %all-to-all-start.1 = ((bf16[16,2,16384]{2,1,0:T(2,128)(2,1)}), bf16[16,2,16384]{2,1,0:T(2,128)(2,1)S(1)}, u32[]{:S(2)}, u32[]{:S(2)}) async-start(bf16[16,2,16384]{2,1,0:T(2,128)(2,1)} %reshape.349), calls=%async_computation.1 | async-start | bytes 2097152 | tf_op jit(solution)/shard_map/all_to_all | solution.py:134
  164.6 8.3 %copy-start.15 = (bf16[1,128,2048]{2,1,0:T(8,128)(2,1)S(1)}, bf16[1,128,2048]{2,1,0:T(8,128)(2,1)}, u32[]{:S(2)}) copy-start(bf16[1,128,2048]{2,1,0:T(8,128)(2,1)} %param.16) | copy-start | bytes 1572868
  164.7 8.3 %copy-start.17 = (f32[2048]{0:T(1024)S(1)}, f32[2048]{0:T(1024)}, u32[]{:S(2)}) copy-start(f32[2048]{0:T(1024)} %param.24) | copy-start | bytes 24580
  242.1 4.9 %copy-start.22 = (f32[1,128,2]{1,2,0:T(2,128)S(1)}, f32[1,128,2]{1,2,0:T(2,128)}, u32[]{:S(2)}) copy-start(f32[1,128,2]{1,2,0:T(2,128)} %param.31) | copy-start | bytes 3076
  242.1 35.1 %all-to-all-start.3 = ((bf16[128,1,1,3,2048]{4,3,2,1,0:T(4,128)(2,1)}), bf16[128,1,1,3,2048]{4,3,2,1,0:T(4,128)(2,1)S(1)}, u32[]{:S(2)}, u32[]{:S(2)}) async-start(bf16[128,1,1,3,2048]{4,3,2,1,0:T(4,128)(2,1)} %bitcast.151), calls=%async_computation.3 | async-start | bytes 4194304 | tf_op jit(solution)/shard_map/all_to_all | solution.py:50
  277.2 1.3 copy-start.4
  287.2 3.3 %copy-start.19 = (f32[2048]{0:T(1024)S(1)}, f32[2048]{0:T(1024)}, u32[]{:S(2)}) copy-start(f32[2048]{0:T(1024)} %param.29) | copy-start | bytes 24580
  (5 other events, 4.7 us)
Sparse Core Ops, SparseCore 0:
  9.0 93.3 all-gather.1
where the time goes:
time: 300 us; the launch traced here: 298 us
  local copies, waits for them, and re-layouts  84.8 us (28%)
  waiting for transfers between devices  81.2 us (27%)
  blocking collectives  38.3 us (13%)
  other arithmetic  36.5 us (12%)
  matrix products  26.5 us (9%)
  starting transfers between devices  17.1 us (6%)
  between operations  14.1 us (5%)
    all_to_all x1, blocking collectives, one_exchange(): lax.all_to_all(pieces, axis, split_axis=0, concat_axis=0, tiled=True)  38.3 us
    all_to_all x1, waiting for transfers between devices, sent_together(): lax.all_to_all(both, axis, split_axis=split_dim, concat_axis=concat_dim,...  37.6 us
    all_to_all x1, waiting for transfers between devices, one_exchange(): lax.all_to_all(pieces, axis, split_axis=0, concat_axis=0, tiled=True)  30.1 us
    pad x6, local copies, waits for them, and re-layouts, block_attention(): lax.associative_scan(combine_states, (decays, updates), axis=0)  23.8 us
    unnamed x56, local copies, waits for them, and re-layouts  20.9 us
    add x5, other arithmetic, block_attention(): lax.associative_scan(combine_states, (decays, updates), axis=0)  12.9 us
    all_to_all x1, waiting for transfers between devices, shards(): lax.all_to_all(normed, 'sp', split_axis=0, concat_axis=1, tiled=True)  12.8 us
    another operation x2, local copies, waits for them, and re-layouts, one_exchange(): pieces = pieces.reshape(-1, *inside)  9.16 us
  transfers between devices with their start and end apart: 4, of which 3 were waited for; matrix products, arithmetic and copies ran while one was open for 30% of the time, Pallas kernels for 0%

commit v1 on v0

v1 whole, which is shorter than its diff:
```python
import jax
import jax.numpy as jnp
from jax import lax
from jax.experimental import pallas as pl
from jax.experimental.pallas import tpu as pltpu
from jax.sharding import PartitionSpec as P

D = 2048
HEADS = 16
DK = 128
DV = 256
TOP = 2
CAP = 3
TOK = 128
FF = 1024
EXTRA_ROWS = 8

EPS = 1e-06
F32 = jnp.float32
BF16 = jnp.bfloat16

NN = (((1,), (0,)), ((), ()))
NT = (((1,), (1,)), ((), ()))
TN = (((0,), (0,)), ((), ()))


def mm(a, b, dims=NN):
    return lax.dot_general(a, b, dims, preferred_element_type=F32)


def params(mib=48):
    return pltpu.CompilerParams(vmem_limit_bytes=mib * 2**20)


def cost(flops, nbytes, trans=0):
    return pl.CostEstimate(flops=flops, bytes_accessed=nbytes, transcendentals=trans)


def lower_ones(n):
    return (
        lax.broadcasted_iota(jnp.int32, (n, n), 0) >= lax.broadcasted_iota(jnp.int32, (n, n), 1)
    )


def three_parts(x):
    a = x.astype(BF16)
    r = x - a.astype(F32)
    b = r.astype(BF16)
    c = (r - b.astype(F32)).astype(BF16)
    return a, b, c


def extra_sums(ex):
    low = lower_ones(TOK).astype(BF16)
    parts = three_parts(ex)
    rows = sum(mm(p, low, NT) for p in parts)
    cols = sum(mm(low, p, NT) for p in parts)
    return rows, cols


def prep_kernel(q_ref, k_ref, g_ref, qd_ref, kd_ref, p_ref, bend_ref):
    x = g_ref[...].astype(F32)
    ls = (jnp.minimum(x, 0.0) - jnp.log1p(jnp.exp(-jnp.abs(x)))) * (1.0 / 16.0)
    low = lower_ones(TOK).astype(BF16)
    hi = ls.astype(BF16)
    lo = (ls - hi.astype(F32)).astype(BF16)
    b = mm(low, hi) + mm(low, lo)
    end = b[TOK - 1 : TOK, :]
    k = k_ref[...].astype(F32)
    qd = (q_ref[...].astype(F32) * (DK**-0.5) * jnp.exp(b)).astype(BF16)
    kp = (k * jnp.exp(-b)).astype(BF16)
    qd_ref[...] = qd
    kd_ref[...] = k * jnp.exp(end - b)
    bend_ref[...] = end
    for h in range(p_ref.shape[0]):
        at = slice(h * DK, (h + 1) * DK)
        p_ref[h] = mm(qd[:, at], kp[:, at], NT)


def prep(q, k, g):
    step = 4
    wide = pl.BlockSpec((TOK, step * DK), lambda i: (0, i))
    return pl.pallas_call(
        prep_kernel,
        grid=(HEADS // step,),
        in_specs=[wide, wide, wide],
        out_specs=[
            wide,
            wide,
            pl.BlockSpec((step, TOK, TOK), lambda i: (i, 0, 0)),
            pl.BlockSpec((1, step * DK), lambda i: (0, i)),
        ],
        out_shape=[
            jax.ShapeDtypeStruct((TOK, HEADS * DK), BF16),
            jax.ShapeDtypeStruct((TOK, HEADS * DK), F32),
            jax.ShapeDtypeStruct((HEADS, TOK, TOK), F32),
            jax.ShapeDtypeStruct((1, HEADS * DK), F32),
        ],
        compiler_params=params(),
        cost_estimate=cost(2 * 10**9, 4 * 2**20, 2**20),
        name="prep",
    )(q, k, g)


def update_kernel(ex_ref, kd_ref, v_ref, bend_ref, u_ref):
    rows, cols = extra_sums(ex_ref[...])
    w = jnp.exp(cols[TOK - 1 : TOK, :] - cols)
    for h in range(HEADS):
        kd = (kd_ref[:, h * DK : (h + 1) * DK] * w[:, h : h + 1]).astype(BF16)
        u = mm(kd, v_ref[:, h * DV : (h + 1) * DV], TN)
        u_ref[h, 0:DK, :] = u.astype(BF16)
        end = bend_ref[:, h * DK : (h + 1) * DK] + rows[h : h + 1, TOK - 1 : TOK]
        hi = end.astype(BF16)
        lo = (end - hi.astype(F32)).astype(BF16)
        both = jnp.concatenate([hi.astype(F32), lo.astype(F32)], axis=1)
        u_ref[h, DK : DK + EXTRA_ROWS, :] = jnp.broadcast_to(both, (EXTRA_ROWS, DV)).astype(BF16)


def update(ex, kd, v, bend):
    return pl.pallas_call(
        update_kernel,
        out_shape=jax.ShapeDtypeStruct((HEADS, DK + EXTRA_ROWS, DV), BF16),
        compiler_params=params(),
        cost_estimate=cost(2 * 10**9, 3 * 2**20),
        name="update",
    )(ex, kd, v, bend)


def inside_kernel(ex_ref, p_ref, v_ref, o_ref):
    rows, cols = extra_sums(ex_ref[...])
    keep = lower_ones(TOK)
    for h in range(HEADS):
        gap = jnp.minimum(cols[:, h : h + 1] - rows[h : h + 1, :], 0.0)
        a = jnp.where(keep, p_ref[h] * jnp.exp(gap), 0.0).astype(BF16)
        o_ref[:, h * DV : (h + 1) * DV] = mm(a, v_ref[:, h * DV : (h + 1) * DV])


def inside(ex, p, v):
    return pl.pallas_call(
        inside_kernel,
        out_shape=jax.ShapeDtypeStruct((TOK, HEADS * DV), F32),
        compiler_params=params(),
        cost_estimate=cost(4 * 10**9, 4 * 2**20, 2**18),
        name="inside",
    )(ex, p, v)


def prefix_kernel(u_ref, s_ref):
    chunks = u_ref.shape[0]
    tail = u_ref[:, DK : DK + EXTRA_ROWS, :].astype(F32)
    ends = tail[:, 0, 0:DK] + tail[:, 0, DK : 2 * DK]
    keep = jnp.transpose(jnp.exp(ends))
    state = jnp.zeros((DK, DV), F32)
    for m in range(chunks):
        s_ref[m] = state.astype(BF16)
        if m + 1 < chunks:
            state = state * keep[:, m : m + 1] + u_ref[m, 0:DK, :].astype(F32)


def prefix(u):
    return pl.pallas_call(
        prefix_kernel,
        out_shape=jax.ShapeDtypeStruct((u.shape[0], DK, DV), BF16),
        compiler_params=params(),
        cost_estimate=cost(10**8, 2 * 2**20),
        name="prefix",
    )(u)


def heads_kernel(ex_ref, qd_ref, s_ref, o_ref, gain_ref, out_ref):
    _, cols = extra_sums(ex_ref[...])
    grow = jnp.exp(cols)
    for h in range(HEADS):
        at = slice(h * DV, (h + 1) * DV)
        cross = mm(qd_ref[:, h * DK : (h + 1) * DK], s_ref[h])
        o = o_ref[:, at] + cross * grow[:, h : h + 1]
        ms = jnp.mean(o * o, axis=1, keepdims=True)
        out_ref[:, at] = (o * lax.rsqrt(ms + EPS) * gain_ref[:, at]).astype(BF16)


def heads(ex, qd, s, o, gain):
    return pl.pallas_call(
        heads_kernel,
        out_shape=jax.ShapeDtypeStruct((TOK, HEADS * DV), BF16),
        compiler_params=params(),
        cost_estimate=cost(2 * 10**9, 5 * 2**20),
        name="heads",
    )(ex, qd, s, o, gain)


KB = 512


def early_kernel(x_ref, *refs):
    n = (len(refs) - 2)
    w_refs, out_ref, acc_ref = refs[:n], refs[n], refs[n + 1]
    i = pl.program_id(0)

    @pl.when(i == 0)
    def _():
        acc_ref[...] = jnp.zeros_like(acc_ref)

    x = x_ref[...]
    for p in range(n):
        acc_ref[p] += mm(x, w_refs[p][...])

    @pl.when(i == pl.num_programs(0) - 1)
    def _():
        out_ref[...] = acc_ref[...].astype(BF16)


def early(x, ws):
    n = len(ws)
    depth, wide = ws[0].shape
    return pl.pallas_call(
        early_kernel,
        grid=(depth // KB,),
        in_specs=[pl.BlockSpec((TOK, KB), lambda i: (0, i))]
        + [pl.BlockSpec((KB, wide), lambda i: (i, 0))] * n,
        out_specs=pl.BlockSpec((n, TOK, wide), lambda i: (0, 0, 0)),
        out_shape=jax.ShapeDtypeStruct((n, TOK, wide), BF16),
        scratch_shapes=[pltpu.VMEM((n, TOK, wide), F32)],
        compiler_params=params(),
        cost_estimate=cost(2 * TOK * depth * wide * n, 2 * depth * wide * n),
        name="early",
    )(x, *ws)


def late_kernel(place_ref, x_ref, *refs):
    done_ref, skip_ref, g1_ref, g2_ref = refs[0:4]
    res_ref, ein_ref, acc_ref, proj_ref = refs[-4:]
    w_refs = refs[4:-4]
    n = len(w_refs)
    i = pl.program_id(0)

    @pl.when(i == 0)
    def _():
        acc_ref[...] = jnp.zeros_like(acc_ref)

    x = x_ref[...]
    for p in range(n):
        acc_ref[p] += mm(x, w_refs[p][...])

    @pl.when(i == pl.num_programs(0) - 1)
    def _():
        m = done_ref.shape[0]
        for p in range(m):
            proj_ref[place_ref[p]] = done_ref[p].astype(F32)
        for p in range(n):
            proj_ref[place_ref[m + p]] = acc_ref[p].astype(BF16).astype(F32)
        wide = proj_ref.shape[2]
        ms = jnp.zeros((TOK, 1), F32)
        for d in range(m + n):
            pr = proj_ref[d]
            ms += jnp.sum(pr * pr, axis=1, keepdims=True)
        inv = lax.rsqrt(ms * (1.0 / D) + EPS)
        ms = jnp.zeros((TOK, 1), F32)
        for d in range(m + n):
            at = slice(d * wide, (d + 1) * wide)
            r = (skip_ref[:, at].astype(F32) + proj_ref[d] * inv * g1_ref[:, at]).astype(BF16)
            res_ref[:, at] = r
            rf = r.astype(F32)
            proj_ref[d] = rf
            ms += jnp.sum(rf * rf, axis=1, keepdims=True)
        inv = lax.rsqrt(ms * (1.0 / D) + EPS)
        for d in range(m + n):
            at = slice(d * wide, (d + 1) * wide)
            ein_ref[:, at] = (proj_ref[d] * inv * g2_ref[:, at]).astype(BF16)


def late(place, x, done, skip, g1, g2, ws):
    n = len(ws)
    depth, wide = ws[0].shape
    whole2 = lambda i: (0, 0)
    return pl.pallas_call(
        late_kernel,
        grid=(depth // KB,),
        in_specs=[
            pl.BlockSpec(memory_space=pltpu.SMEM),
            pl.BlockSpec((TOK, KB), lambda i: (0, i)),
            pl.BlockSpec(done.shape, lambda i: (0, 0, 0)),
            pl.BlockSpec((TOK, D), whole2),
            pl.BlockSpec((1, D), whole2),
            pl.BlockSpec((1, D), whole2),
        ]
        + [pl.BlockSpec((KB, wide), lambda i: (i, 0))] * n,
        out_specs=[pl.BlockSpec((TOK, D), whole2), pl.BlockSpec((TOK, D), whole2)],
        out_shape=[jax.ShapeDtypeStruct((TOK, D), BF16), jax.ShapeDtypeStruct((TOK, D), BF16)],
        scratch_shapes=[
            pltpu.VMEM((n, TOK, wide), F32),
            pltpu.VMEM((D // wide, TOK, wide), F32),
        ],
        compiler_params=params(),
        cost_estimate=cost(2 * TOK * depth * wide * n, 2 * depth * wide * n),
        name="late",
    )(place, x, done, skip, g1, g2, *ws)


def send_kernel(slot_ref, x_ref, out_ref):
    out_ref[...] = jnp.zeros_like(out_ref)

    def body(t, _):
        row = x_ref[t]
        out_ref[slot_ref[TOP * t]] = row
        out_ref[slot_ref[TOP * t + 1]] = row
        return 0

    lax.fori_loop(0, TOK, body, 0, unroll=8)


def send_rows(slots, x3, rows):
    return pl.pallas_call(
        send_kernel,
        in_specs=[
            pl.BlockSpec(memory_space=pltpu.SMEM),
            pl.BlockSpec(memory_space=pltpu.VMEM),
        ],
        out_shape=jax.ShapeDtypeStruct((rows, 16, 128), BF16),
        compiler_params=params(),
        cost_estimate=cost(10**6, 2 * 2**20),
        name="send_rows",
    )(slots, x3)


def expert_kernel(x_ref, wg_ref, wu_ref, wd_ref, out_ref, acc_ref):
    i = pl.program_id(0)
    x = x_ref[...]
    gate = mm(x, wg_ref[...])
    up = mm(x, wu_ref[...])
    hid = (gate * jax.nn.sigmoid(gate) * up).astype(BF16)
    part = mm(hid, wd_ref[...])

    @pl.when(i == 0)
    def _():
        acc_ref[...] = part

    @pl.when((i > 0) & (i < pl.num_programs(0) - 1))
    def _():
        acc_ref[...] += part

    @pl.when(i == pl.num_programs(0) - 1)
    def _():
        out_ref[...] = (acc_ref[...] + part).astype(BF16)


def experts(x, wg, wu, wd):
    rows = x.shape[0]
    fb = 256
    return pl.pallas_call(
        expert_kernel,
        grid=(FF // fb,),
        in_specs=[
            pl.BlockSpec((rows, D), lambda i: (0, 0)),
            pl.BlockSpec((D, fb), lambda i: (0, i)),
            pl.BlockSpec((D, fb), lambda i: (0, i)),
            pl.BlockSpec((fb, D), lambda i: (i, 0)),
        ],
        out_specs=pl.BlockSpec((rows, D), lambda i: (0, 0)),
        out_shape=jax.ShapeDtypeStruct((rows, D), BF16),
        scratch_shapes=[pltpu.VMEM((rows, D), F32)],
        compiler_params=params(),
        cost_estimate=cost(6 * rows * D * FF, 6 * D * FF),
        name="experts",
    )(x, wg, wu, wd)


def combine_kernel(slot_ref, w_ref, back_ref, res_ref, gain_ref, out_ref):
    gain = gain_ref[...]

    def body(i, _):
        for j in range(8):
            t = i * 8 + j
            a = back_ref[slot_ref[TOP * t]].astype(F32) * w_ref[TOP * t]
            b = back_ref[slot_ref[TOP * t + 1]].astype(F32) * w_ref[TOP * t + 1]
            c = a + b
            ms = jnp.sum(c * c, keepdims=True).reshape(1, 1) * (1.0 / D)
            out_ref[t] = (res_ref[t].astype(F32) + c * lax.rsqrt(ms + EPS) * gain).astype(BF16)
        return 0

    lax.fori_loop(0, TOK // 8, body, 0)


def combine(slots, weights, back, res3, gain):
    smem = pl.BlockSpec(memory_space=pltpu.SMEM)
    vmem = pl.BlockSpec(memory_space=pltpu.VMEM)
    return pl.pallas_call(
        combine_kernel,
        in_specs=[smem, smem, vmem, vmem, vmem],
        out_shape=jax.ShapeDtypeStruct((TOK, 16, 128), BF16),
        compiler_params=params(),
        cost_estimate=cost(10**7, 3 * 2**20),
        name="combine",
    )(slots, weights, back, res3, gain)


def shards(
    skip_stream_entering,
    mapped_probe_matrix,
    mapped_lookup_matrix,
    mapped_content_matrix,
    retention_preactivation,
    extra_shrinkage,
    attention_group_scale,
    final_projection_matrix,
    blender_branch_scale,
    specialist_prenormal_scale,
    specialist_switch_matrix,
    specialist_expand_matrix,
    specialist_contract_matrix,
    specialist_branch_scale,
    assigned_specialists,
    dispatcher_logits,
):
    sp_count = lax.axis_size("sp")
    dp_count = lax.axis_size("dp")
    total = sp_count * dp_count

    core = lax.axis_index("dp") % 2
    ychip = lax.axis_index("dp") // 2
    ychips = dp_count // 2

    def ring(sign):
        out = []
        for d in range(dp_count):
            y, c = d // 2, d % 2
            s = sign if c == 0 else -sign
            out.append((d, ((y + s) % ychips) * 2 + c))
        return out

    swap = [(d, d ^ 1) for d in range(dp_count)]
    w_own = final_projection_matrix
    w_a = lax.ppermute(w_own, "dp", ring(1))
    w_b = lax.ppermute(w_own, "dp", ring(-1))
    w_own_s = lax.ppermute(w_own, "dp", swap)

    q = mapped_probe_matrix[0]
    k = mapped_lookup_matrix[0]
    v = mapped_content_matrix[0]
    g = retention_preactivation[0]
    ex = lax.all_to_all(
        extra_shrinkage[0].reshape(sp_count, 1, TOK), "sp", split_axis=0, concat_axis=0, tiled=True
    ).reshape(HEADS, TOK)
    qd, kd, p, bend = prep(q, k, g)
    u = update(ex, kd, v, bend)
    u_in = lax.all_to_all(u, "sp", split_axis=0, concat_axis=0, tiled=True)
    o_in = inside(ex, p, v)
    s = prefix(u_in)
    s_in = lax.all_to_all(s, "sp", split_axis=0, concat_axis=0, tiled=True)

    w_a_f, _ = lax.optimization_barrier((w_a, s))
    w_a2 = lax.ppermute(w_a_f, "dp", ring(1))
    w_a_s = lax.ppermute(w_a_f, "dp", swap)
    w_b_s = lax.ppermute(w_b, "dp", swap)
    w_a2_s = lax.ppermute(w_a2, "dp", swap)

    head_out = heads(ex, qd, s_in, o_in, attention_group_scale.reshape(1, HEADS * DV))

    sgn = 1 - 2 * core
    y_a = (ychip - sgn) % ychips
    y_b = (ychip + sgn) % ychips
    y_a2 = (ychip - 2 * sgn) % ychips
    y_as = (ychip + sgn) % ychips
    y_bs = (ychip - sgn) % ychips
    other = 1 - core
    place = jnp.stack(
        [
            ychip * 2 + core,
            ychip * 2 + other,
            y_a * 2 + core,
            y_as * 2 + other,
            y_b * 2 + core,
            y_bs * 2 + other,
            y_a2 * 2 + core,
            y_a2 * 2 + other,
        ]
    ).astype(jnp.int32)
    done = early(head_out, [w_own, w_own_s, w_a, w_a_s, w_b, w_b_s])
    residual, expert_in = late(
        place,
        head_out,
        done,
        skip_stream_entering[0],
        blender_branch_scale.reshape(1, D),
        specialist_prenormal_scale.reshape(1, D),
        [w_a2, w_a2_s],
    )

    chosen = assigned_specialists[0].reshape(-1)
    onehot = (chosen[:, None] == jnp.arange(total, dtype=jnp.int32)[None, :]).astype(jnp.int32)
    ranks = jnp.sum((jnp.cumsum(onehot, axis=0) - onehot) * onehot, axis=1)
    slots = chosen * CAP + ranks
    weights = dispatcher_logits[0]
    weights = (weights / jnp.sum(weights, axis=1, keepdims=True)).reshape(-1)

    outgoing = send_rows(slots, expert_in.reshape(TOK, 16, 128), total * CAP)
    arrived = lax.all_to_all(
        outgoing.reshape(total, CAP, 16, 128),
        ("sp", "dp"),
        split_axis=0,
        concat_axis=0,
        tiled=True,
    )
    result = experts(
        arrived.reshape(total * CAP, D),
        specialist_switch_matrix[0],
        specialist_expand_matrix[0],
        specialist_contract_matrix[0],
    )
    back = lax.all_to_all(
        result.reshape(total, CAP, 16, 128),
        ("sp", "dp"),
        split_axis=0,
        concat_axis=0,
        tiled=True,
    ).reshape(total * CAP, 16, 128)
    out = combine(
        slots,
        weights,
        back,
        residual.reshape(TOK, 16, 128),
        specialist_branch_scale.reshape(16, 128),
    )
    return out.reshape(1, TOK, D)


def solution(mesh):
    return jax.shard_map(
        shards,
        mesh=mesh,
        in_specs=(
            P("dp", "sp", None),
            P("dp", "sp", None),
            P("dp", "sp", None),
            P("dp", "sp", None),
            P("dp", "sp", None),
            P("dp", "sp", None),
            P(),
            P(None, "dp"),
            P(),
            P(),
            P(("sp", "dp"), None, None),
            P(("sp", "dp"), None, None),
            P(("sp", "dp"), None, None),
            P(),
            P("dp", "sp", None),
            P("dp", "sp", None),
        ),
        out_specs=P("dp", "sp", None),
        check_vma=False,
    )
```

time: 300 us -> 195 us (0.65)
  local copies, waits for them, and re-layouts: 84.8 us -> 14.7 us
  other arithmetic: 36.5 us -> 0.47 us
  Pallas kernels: 0 us -> 35.9 us
  matrix products: 26.5 us -> 0 us
  starting transfers between devices: 17.1 us -> 35.7 us
  between operations: 14.1 us -> 0.39 us
  blocking collectives: 38.3 us -> 29.4 us
  waiting for transfers between devices: 81.2 us -> 78 us
    pallas_call x0 -> x10, Pallas kernels: none -> 35.9 us  [the longest x1 8.95 us: experts(): pl.pallas_call(expert_kernel, grid=(FF // fb,), in_specs=[pl.BlockSpec((r...]
    dot_general x6 -> x0, matrix products: 26.5 us -> none  [the longest x1 8.57 us: shards(): jnp.dot(hidden_units, specialist_contract_matrix[0], preferred_element_ty...]
    all_to_all x3 -> x4, waiting for transfers between devices: 80.5 us -> 54.1 us  [the longest x1 23.9 us: shards(): lax.all_to_all(result.reshape(total, CAP, 16, 128), ('sp', 'dp'), split_a...]
    ppermute x0 -> x7, waiting for transfers between devices: none -> 23.8 us  [the longest x1 17.6 us: shards(): w_a2 = lax.ppermute(w_a_f, 'dp', ring(1))]
    pad x6 -> x0, local copies, waits for them, and re-layouts: 23.8 us -> none  [block_attention(): lax.associative_scan(combine_states, (decays, updates), axis=0)]
    add x13 -> x1, other arithmetic: 18 us -> 0.01 us  [shards(): slots = chosen * CAP + ranks]
    another operation x12 -> x5, local copies, waits for them, and re-layouts: 17.8 us -> 0.24 us  [the longest x1 0.14 us: shards(): chosen = assigned_specialists[0].reshape(-1)]
    ppermute x0 -> x7, starting transfers between devices: none -> 9.77 us  [the longest x1 3.6 us: shards(): w_b_s = lax.ppermute(w_b, 'dp', swap)]
  transfers between devices with their start and end apart: 4 -> 11, of which waited for: 3 -> 5; matrix products, arithmetic and copies ran while one was open for 30% -> 1% of each run, Pallas kernels for 0% -> 9%
where the time goes in v1:
time: 195 us; the launch traced here: 194 us
  waiting for transfers between devices  78 us (40%)
  Pallas kernels  35.9 us (18%)
  starting transfers between devices  35.7 us (18%)
  blocking collectives  29.4 us (15%)
  local copies, waits for them, and re-layouts  14.7 us (8%)
    all_to_all x1, blocking collectives, shards(): lax.all_to_all(outgoing.reshape(total, CAP, 16, 128), ('sp', 'dp'), split...  29.4 us
    all_to_all x1, waiting for transfers between devices, shards(): lax.all_to_all(result.reshape(total, CAP, 16, 128), ('sp', 'dp'), split_a...  23.9 us
    all_to_all x1, waiting for transfers between devices, shards(): u_in = lax.all_to_all(u, 'sp', split_axis=0, concat_axis=0, tiled=True)  18 us
    ppermute x1, waiting for transfers between devices, shards(): w_a2 = lax.ppermute(w_a_f, 'dp', ring(1))  17.6 us
    unnamed x43, local copies, waits for them, and re-layouts  12.8 us
    all_to_all x1, waiting for transfers between devices, shards(): s_in = lax.all_to_all(s, 'sp', split_axis=0, concat_axis=0, tiled=True)  12.3 us
    pallas_call x1, Pallas kernels, experts(): pl.pallas_call(expert_kernel, grid=(FF // fb,), in_specs=[pl.BlockSpec((r...  8.95 us
    pallas_call x1, Pallas kernels, early(): pl.pallas_call(early_kernel, grid=(depth // KB,), in_specs=[pl.BlockSpec(...  7.95 us
  transfers between devices with their start and end apart: 11, of which 5 were waited for; matrix products, arithmetic and copies ran while one was open for 1% of the time, Pallas kernels for 9%

profile of v1, /device:TPU:1, one launch (start us, length us, event | category | flops | bytes accessed | tf_op | source)
XLA Modules:
  0.0 194.4 jit_solution(11801214354535391160)
XLA Ops:
  0.0 3.6 %collective-permute-start.1 = (bf16[4096,256]{1,0:T(8,128)(2,1)}, bf16[4096,256]{1,0:T(8,128)(2,1)}, u32[]{:S(2)}, u32[]{:S(2)}) collective-permute-start(bf16[4096,256]{1,0:T(8,128)(2,1)} %refs_0_.1), channel_id=1, source_target_pairs={{0,2},{1,7},{2,4},{3,1},{4,6},{5,3},{6,0},{7,5},{8,10},{9,15},{10,... | collective-permute-start | bytes 6291464 | tf_op jit(solution)/shard_map/ppermute | solution.py:432
  3.6 7.6 %all-to-all-start = ((f32[16,1,128]{2,1,0:T(1,128)}), f32[16,1,128]{2,1,0:T(1,128)S(1)}, u32[]{:S(2)}, u32[]{:S(2)}) async-start(f32[16,1,128]{2,1,0:T(1,128)} %bitcast.75), calls=%async_computation | async-start | bytes 16384 | tf_op jit(solution)/shard_map/all_to_all | solution.py:440
  14.3 2.7 %prep.1 = (bf16[128,2048]{1,0:T(8,128)(2,1)S(1)}, f32[128,2048]{1,0:T(8,128)S(1)}, f32[16,128,128]{2,1,0:T(8,128)S(1)}, f32[1,2048]{1,0:T(1,128)S(1)}) custom-call(bf16[128,2048]{1,0:T(8,128)(2,1)S(1)} %bitcast.66, bf16[128,2048]{1,0:T(8,128)(2,1)S(1)} %bitcast.67, bf16[128,2048]{1,0:T(8,128)(2,1)S(1)} %bitcast.68), custom_call_target="tpu_custom_call" | custom-call | flops 2000000000 | bytes 4194304 | tf_op jit(solution)/shard_map/prep/pallas_call | solution.py:83
  17.8 2.1 %update.1 = bf16[16,136,256]{2,1,0:T(8,128)(2,1)} custom-call(f32[16,128]{1,0:T(8,128)S(1)} %bitcast.61, f32[128,2048]{1,0:T(8,128)S(1)} %get-tuple-element.13.kd_ref, bf16[128,4096]{1,0:T(8,128)(2,1)S(1)} %bitcast.64, f32[1,2048]{1,0:T(1,128)S(1)} %get-tuple-element.14.bend_ref), custom_call_target="tpu_custom_call" | custom-call | flops 2000000000 | bytes 3145728 | tf_op jit(solution)/shard_map/update/pallas_call | solution.py:120
  19.9 6.8 %all-to-all-start.1 = ((bf16[16,136,256]{2,1,0:T(8,128)(2,1)}), bf16[16,136,256]{2,1,0:T(8,128)(2,1)S(1)}, u32[]{:S(2)}, u32[]{:S(2)}) async-start(bf16[16,136,256]{2,1,0:T(8,128)(2,1)} %update.1), calls=%async_computation.1 | async-start | bytes 2228224 | tf_op jit(solution)/shard_map/all_to_all | solution.py:445
  26.8 18.0 %all-to-all-done.1.u_ref = bf16[16,136,256]{2,1,0:T(8,128)(2,1)S(1)} async-done(((bf16[16,136,256]{2,1,0:T(8,128)(2,1)}), bf16[16,136,256]{2,1,0:T(8,128)(2,1)S(1)}, u32[]{:S(2)}, u32[]{:S(2)}) %all-to-all-start.1) | async-done | bytes 1114144 | tf_op jit(solution)/shard_map/all_to_all | solution.py:445
  44.8 1.5 prefix.1
  46.3 1.7 collective-permute-start
  48.0 6.2 %collective-permute-done.3.refs_4_ = bf16[4096,256]{1,0:T(8,128)(2,1)} collective-permute-done((bf16[4096,256]{1,0:T(8,128)(2,1)}, bf16[4096,256]{1,0:T(8,128)(2,1)}, u32[]{:S(2)}, u32[]{:S(2)}) %collective-permute-start.3) | collective-permute-done | bytes 2097184 | tf_op jit(solution)/shard_map/ppermute | solution.py:433
  54.2 3.6 %collective-permute-start.4 = (bf16[4096,256]{1,0:T(8,128)(2,1)}, bf16[4096,256]{1,0:T(8,128)(2,1)}, u32[]{:S(2)}, u32[]{:S(2)}) collective-permute-start(bf16[4096,256]{1,0:T(8,128)(2,1)} %collective-permute-done.3.refs_4_), channel_id=1, source_target_pairs={{0,1},{1,0},{2,3},{3,2},{4,5},{5,4},{6,7},{7,6},{8,9},{9,8},{10,11... | collective-permute-start | bytes 6291464 | tf_op jit(solution)/shard_map/ppermute | solution.py:453
  57.8 17.6 %collective-permute-done.5.refs_4_ = bf16[4096,256]{1,0:T(8,128)(2,1)S(1)} collective-permute-done((bf16[4096,256]{1,0:T(8,128)(2,1)}, bf16[4096,256]{1,0:T(8,128)(2,1)S(1)}, u32[]{:S(2)}, u32[]{:S(2)}) %collective-permute-start.5) | collective-permute-done | bytes 2097184 | tf_op jit(solution)/shard_map/ppermute | solution.py:451
  76.8 6.6 %all-to-all-start.2 = ((bf16[16,128,256]{2,1,0:T(8,128)(2,1)}), bf16[16,128,256]{2,1,0:T(8,128)(2,1)S(1)}, u32[]{:S(2)}, u32[]{:S(2)}) async-start(bf16[16,128,256]{2,1,0:T(8,128)(2,1)} %prefix.1), calls=%async_computation.2 | async-start | bytes 2097152 | tf_op jit(solution)/shard_map/all_to_all | solution.py:448
  87.3 1.3 copy-done.10
  88.6 12.3 %all-to-all-done.2.s_ref = bf16[16,128,256]{2,1,0:T(8,128)(2,1)S(1)} async-done(((bf16[16,128,256]{2,1,0:T(8,128)(2,1)}), bf16[16,128,256]{2,1,0:T(8,128)(2,1)S(1)}, u32[]{:S(2)}, u32[]{:S(2)}) %all-to-all-start.2) | async-done | bytes 1048608 | tf_op jit(solution)/shard_map/all_to_all | solution.py:448
  100.8 1.6 copy-done.11
  103.5 1.7 heads.1.x_ref
  105.3 7.9 %early.1.refs_0_ = bf16[6,128,256]{2,1,0:T(8,128)(2,1)S(1)} custom-call(bf16[128,4096]{1,0:T(8,128)(2,1)S(1)} %heads.1.x_ref, bf16[4096,256]{1,0:T(8,128)(2,1)} %refs_0_.1, bf16[4096,256]{1,0:T(8,128)(2,1)} %collective-permute-done.refs_1_, bf16[4096,256]{1,0:T(8,128)(2,1)} %collective-permute-done.1.refs_2_, ...), custom_call_target="tpu_custom_call" | custom-call | flops 1610612736 | bytes 12582912 | tf_op jit(solution)/shard_map/early/pallas_call | solution.py:215
  113.3 6.0 %late.1 = (bf16[128,2048]{1,0:T(8,128)(2,1)S(1)}, bf16[128,2048]{1,0:T(8,128)(2,1)S(1)}) custom-call(s32[8]{0:T(128)S(1)} %stack.35.place_ref, bf16[128,4096]{1,0:T(8,128)(2,1)S(1)} %heads.1.x_ref, bf16[6,128,256]{2,1,0:T(8,128)(2,1)S(1)} %early.1.refs_0_, bf16[128,2048]{1,0:T(8,128)(2,1)S(1)} %bitcast.55, f32[1,2048]{1,0:T(1,128)S(1)} %bitcast.58, ...), custom_call_target="tpu_custom_call" | custom-call | flops 536870912 | bytes 4194304 | tf_op jit(solution)/shard_map/late/pallas_call | solution.py:275
  120.5 29.4 %all_to_all.25 = bf16[128,3,16,128]{3,2,1,0:T(8,128)(2,1)S(1)} all-to-all(bf16[128,3,16,128]{3,2,1,0:T(8,128)(2,1)S(1)} %bitcast.50), channel_id=1, replica_groups=mesh['sp'=16,'dp'=8] {'sp','dp'}, dimensions={0} | all-to-all | bytes 3145728 | tf_op jit(solution)/shard_map/all_to_all | solution.py:496
  150.3 8.9 %experts.1 = bf16[384,2048]{1,0:T(8,128)(2,1)S(1)} custom-call(bf16[384,2048]{1,0:T(8,128)(2,1)S(1)} %bitcast.53, bf16[2048,1024]{1,0:T(8,128)(2,1)} %bitcast.76, bf16[2048,1024]{1,0:T(8,128)(2,1)} %bitcast.77, bf16[1024,2048]{1,0:T(8,128)(2,1)} %bitcast.78), custom_call_target="tpu_custom_call" | custom-call | flops 4831838208 | bytes 12582912 | tf_op jit(solution)/shard_map/experts/pallas_call | solution.py:349
  159.3 1.6 copy.29
  160.9 5.0 %all-to-all-start.4 = ((bf16[128,3,16,128]{3,2,1,0:T(8,128)(2,1)}), bf16[128,3,16,128]{3,2,1,0:T(8,128)(2,1)S(1)}, u32[]{:S(2)}, u32[]{:S(2)}) async-start(bf16[128,3,16,128]{3,2,1,0:T(8,128)(2,1)} %bitcast.70), calls=%async_computation.4 | async-start | bytes 3145728 | tf_op jit(solution)/shard_map/all_to_all | solution.py:509
  166.5 23.9 %all-to-all-done.4 = bf16[128,3,16,128]{3,2,1,0:T(8,128)(2,1)S(1)} async-done(((bf16[128,3,16,128]{3,2,1,0:T(8,128)(2,1)}), bf16[128,3,16,128]{3,2,1,0:T(8,128)(2,1)S(1)}, u32[]{:S(2)}, u32[]{:S(2)}) %all-to-all-start.4) | async-done | bytes 1572896 | tf_op jit(solution)/shard_map/all_to_all | solution.py:509
  190.4 3.1 %combine.1 = bf16[128,16,128]{2,1,0:T(8,128)(2,1)S(1)} custom-call(s32[256]{0:T(256)S(1)} %multiply_add_fusion.slot_ref, f32[256]{0:T(256)S(1)} %div.21.w_ref, bf16[384,16,128]{2,1,0:T(8,128)(2,1)S(1)} %bitcast.49, bf16[128,16,128]{2,1,0:T(8,128)(2,1)S(1)} %bitcast.51, f32[16,128]{1,0:T(8,128)S(1)} %bitcast.60), custom_call_target="tpu_custom_call" | custom-call | flops 10000000 | bytes 3145728 | tf_op jit(solution)/shard_map/combine/pallas_call | solution.py:386
  (70 shorter events, 13.5 us)
Async XLA Ops:
  0.0 46.3 %collective-permute-start.1 = (bf16[4096,256]{1,0:T(8,128)(2,1)}, bf16[4096,256]{1,0:T(8,128)(2,1)}, u32[]{:S(2)}, u32[]{:S(2)}) collective-permute-start(bf16[4096,256]{1,0:T(8,128)(2,1)} %refs_0_.1), channel_id=1, source_target_pairs={{0,2},{1,7},{2,4},{3,1},{4,6},{5,3},{6,0},{7,5},{8,10},{9,15},{10,... | collective-permute-start | bytes 6291464 | tf_op jit(solution)/shard_map/ppermute | solution.py:432
  3.6 14.2 %all-to-all-start = ((f32[16,1,128]{2,1,0:T(1,128)}), f32[16,1,128]{2,1,0:T(1,128)S(1)}, u32[]{:S(2)}, u32[]{:S(2)}) async-start(f32[16,1,128]{2,1,0:T(1,128)} %bitcast.75), calls=%async_computation | async-start | bytes 16384 | tf_op jit(solution)/shard_map/all_to_all | solution.py:440
  14.3 3.5 %copy-start.4 = (bf16[1,128,4096]{2,1,0:T(8,128)(2,1)S(1)}, bf16[1,128,4096]{2,1,0:T(8,128)(2,1)}, u32[]{:S(2)}) copy-start(bf16[1,128,4096]{2,1,0:T(8,128)(2,1)} %param.19) | copy-start | bytes 3145732
  17.8 2.1 %copy-start.14 = (f32[16,128,128]{2,1,0:T(8,128)}, f32[16,128,128]{2,1,0:T(8,128)S(1)}, u32[]{:S(2)}) copy-start(f32[16,128,128]{2,1,0:T(8,128)S(1)} %get-tuple-element.15.p_ref) | copy-start | bytes 3145732
  19.9 56.3 %copy-start.17 = (s32[1,128,2]{1,2,0:T(2,128)S(1)}, s32[1,128,2]{1,2,0:T(2,128)}, u32[]{:S(2)}) copy-start(s32[1,128,2]{1,2,0:T(2,128)} %param.30) | copy-start | bytes 3076
  19.9 24.9 %all-to-all-start.1 = ((bf16[16,136,256]{2,1,0:T(8,128)(2,1)}), bf16[16,136,256]{2,1,0:T(8,128)(2,1)S(1)}, u32[]{:S(2)}, u32[]{:S(2)}) async-start(bf16[16,136,256]{2,1,0:T(8,128)(2,1)} %update.1), calls=%async_computation.1 | async-start | bytes 2228224 | tf_op jit(solution)/shard_map/all_to_all | solution.py:445
  26.7 27.5 %collective-permute-start.3 = (bf16[4096,256]{1,0:T(8,128)(2,1)}, bf16[4096,256]{1,0:T(8,128)(2,1)}, u32[]{:S(2)}, u32[]{:S(2)}) collective-permute-start(bf16[4096,256]{1,0:T(8,128)(2,1)} %refs_0_.1), channel_id=1, source_target_pairs={{0,6},{1,3},{2,0},{3,5},{4,2},{5,7},{6,4},{7,1},{8,14},{9,11},{10,... | collective-permute-start | bytes 6291464 | tf_op jit(solution)/shard_map/ppermute | solution.py:433
  46.3 29.2 %collective-permute-start.5 = (bf16[4096,256]{1,0:T(8,128)(2,1)}, bf16[4096,256]{1,0:T(8,128)(2,1)S(1)}, u32[]{:S(2)}, u32[]{:S(2)}) collective-permute-start(bf16[4096,256]{1,0:T(8,128)(2,1)} %collective-permute-done.1.refs_2_), channel_id=1, source_target_pairs={{0,2},{1,7},{2,4},{3,1},{4,6},{5,3},{6,0},{7,5},{8,10},{9,15},{10,... | collective-permute-start | bytes 6291464 | tf_op jit(solution)/shard_map/ppermute | solution.py:451
  46.3 59.0 %collective-permute-start = (bf16[4096,256]{1,0:T(8,128)(2,1)}, bf16[4096,256]{1,0:T(8,128)(2,1)}, u32[]{:S(2)}, u32[]{:S(2)}) collective-permute-start(bf16[4096,256]{1,0:T(8,128)(2,1)} %refs_0_.1), channel_id=1, source_target_pairs={{0,1},{1,0},{2,3},{3,2},{4,5},{5,4},{6,7},{7,6},{8,9},{9,8},{10,11... | collective-permute-start | bytes 6291464 | tf_op jit(solution)/shard_map/ppermute | solution.py:434
  48.0 57.3 %collective-permute-start.2 = (bf16[4096,256]{1,0:T(8,128)(2,1)}, bf16[4096,256]{1,0:T(8,128)(2,1)}, u32[]{:S(2)}, u32[]{:S(2)}) collective-permute-start(bf16[4096,256]{1,0:T(8,128)(2,1)} %collective-permute-done.1.refs_2_), channel_id=1, source_target_pairs={{0,1},{1,0},{2,3},{3,2},{4,5},{5,4},{6,7},{7,6},{8,9},{9,8},{10,11... | collective-permute-start | bytes 6291464 | tf_op jit(solution)/shard_map/ppermute | solution.py:452
  54.2 51.0 %collective-permute-start.4 = (bf16[4096,256]{1,0:T(8,128)(2,1)}, bf16[4096,256]{1,0:T(8,128)(2,1)}, u32[]{:S(2)}, u32[]{:S(2)}) collective-permute-start(bf16[4096,256]{1,0:T(8,128)(2,1)} %collective-permute-done.3.refs_4_), channel_id=1, source_target_pairs={{0,1},{1,0},{2,3},{3,2},{4,5},{5,4},{6,7},{7,6},{8,9},{9,8},{10,11... | collective-permute-start | bytes 6291464 | tf_op jit(solution)/shard_map/ppermute | solution.py:453
  75.5 37.8 %collective-permute-start.6 = (bf16[4096,256]{1,0:T(8,128)(2,1)S(1)}, bf16[4096,256]{1,0:T(8,128)(2,1)}, u32[]{:S(2)}, u32[]{:S(2)}) collective-permute-start(bf16[4096,256]{1,0:T(8,128)(2,1)S(1)} %collective-permute-done.5.refs_4_), channel_id=1, source_target_pairs={{0,1},{1,0},{2,3},{3,2},{4,5},{5,4},{6,7},{7,6},{8,9},{9,8},{10,11... | collective-permute-start | bytes 6291464 | tf_op jit(solution)/shard_map/ppermute | solution.py:454
  76.8 24.0 %all-to-all-start.2 = ((bf16[16,128,256]{2,1,0:T(8,128)(2,1)}), bf16[16,128,256]{2,1,0:T(8,128)(2,1)S(1)}, u32[]{:S(2)}, u32[]{:S(2)}) async-start(bf16[16,128,256]{2,1,0:T(8,128)(2,1)} %prefix.1), calls=%async_computation.2 | async-start | bytes 2097152 | tf_op jit(solution)/shard_map/all_to_all | solution.py:448
  84.1 1.2 copy-start.5
  85.3 1.2 copy-start.15
  86.5 14.3 %copy-start.9 = (f32[4096]{0:T(1024)S(1)}, f32[4096]{0:T(1024)}, u32[]{:S(2)}) copy-start(f32[4096]{0:T(1024)} %param.22) | copy-start | bytes 49156
  87.3 1.3 copy-start.10
  100.8 1.6 copy-start.11
  105.2 8.0 %copy-start = (bf16[1,128,2048]{2,1,0:T(8,128)(2,1)S(1)}, bf16[1,128,2048]{2,1,0:T(8,128)(2,1)}, u32[]{:S(2)}) copy-start(bf16[1,128,2048]{2,1,0:T(8,128)(2,1)} %param.16) | copy-start | bytes 1572868
  105.2 8.0 %copy-start.1 = (f32[2048]{0:T(1024)S(1)}, f32[2048]{0:T(1024)}, u32[]{:S(2)}) copy-start(f32[2048]{0:T(1024)} %param.24) | copy-start | bytes 24580
  105.2 8.0 %copy-start.2 = (f32[2048]{0:T(1024)S(1)}, f32[2048]{0:T(1024)}, u32[]{:S(2)}) copy-start(f32[2048]{0:T(1024)} %param.25) | copy-start | bytes 24580
  160.9 5.0 %copy-start.16 = (f32[1,128,2]{1,2,0:T(2,128)S(1)}, f32[1,128,2]{1,2,0:T(2,128)}, u32[]{:S(2)}) copy-start(f32[1,128,2]{1,2,0:T(2,128)} %param.31) | copy-start | bytes 3076
  160.9 29.5 %copy-start.3 = (f32[2048]{0:T(1024)S(1)}, f32[2048]{0:T(1024)}, u32[]{:S(2)}) copy-start(f32[2048]{0:T(1024)} %param.29) | copy-start | bytes 24580
  160.9 29.5 %all-to-all-start.4 = ((bf16[128,3,16,128]{3,2,1,0:T(8,128)(2,1)}), bf16[128,3,16,128]{3,2,1,0:T(8,128)(2,1)S(1)}, u32[]{:S(2)}, u32[]{:S(2)}) async-start(bf16[128,3,16,128]{3,2,1,0:T(8,128)(2,1)} %bitcast.70), calls=%async_computation.4 | async-start | bytes 3145728 | tf_op jit(solution)/shard_map/all_to_all | solution.py:509
  (5 other events, 5.0 us)

commit v2 on v1

v2 whole, which is shorter than its diff:
```python
import jax
import jax.numpy as jnp
from jax import lax
from jax.experimental import pallas as pl
from jax.experimental.pallas import tpu as pltpu
from jax.sharding import PartitionSpec as P


D = 2048
HEADS = 16
DK = 128
DV = 256
TOP = 2
CAP = 3
TOK = 128
FF = 1024
EXTRA_ROWS = 8

EPS = 1e-06
F32 = jnp.float32
BF16 = jnp.bfloat16

NN = (((1,), (0,)), ((), ()))
NT = (((1,), (1,)), ((), ()))
TN = (((0,), (0,)), ((), ()))


def mm(a, b, dims=NN):
    return lax.dot_general(a, b, dims, preferred_element_type=F32)


def params(mib):
    return pltpu.CompilerParams(vmem_limit_bytes=mib * 2**20)


def cost(flops, nbytes, trans=0):
    return pl.CostEstimate(flops=flops, bytes_accessed=nbytes, transcendentals=trans)


def lower_ones(n):
    return (
        lax.broadcasted_iota(jnp.int32, (n, n), 0) >= lax.broadcasted_iota(jnp.int32, (n, n), 1)
    )


def three_parts(x):
    a = x.astype(BF16)
    r = x - a.astype(F32)
    b = r.astype(BF16)
    c = (r - b.astype(F32)).astype(BF16)
    return a, b, c


def extra_sums(ex):
    low = lower_ones(TOK).astype(BF16)
    parts = three_parts(ex)
    rows = sum(mm(p, low, NT) for p in parts)
    cols = sum(mm(low, p, NT) for p in parts)
    return rows, cols


def prep_kernel(q_hbm, k_hbm, g_hbm, qd_ref, kd_ref, p_ref, bend_ref, q_ref, k_ref, g_ref, sems):
    parts = 4
    wide = HEADS * DK // parts
    low = lower_ones(TOK).astype(BF16)

    def moves(i):
        at = slice(i * wide, (i + 1) * wide)
        return [
            pltpu.make_async_copy(src.at[:, at], dst.at[:, at], sems.at[i, n])
            for n, (src, dst) in enumerate(((g_hbm, g_ref), (k_hbm, k_ref), (q_hbm, q_ref)))
        ]

    for i in range(parts):
        for m in moves(i):
            m.start()
    for i in range(parts):
        for m in moves(i):
            m.wait()
        at = slice(i * wide, (i + 1) * wide)
        x = g_ref[:, at].astype(F32)
        ls = (jnp.minimum(x, 0.0) - jnp.log1p(jnp.exp(-jnp.abs(x)))) * (1.0 / 16.0)
        hi = ls.astype(BF16)
        lo = (ls - hi.astype(F32)).astype(BF16)
        b = mm(low, hi) + mm(low, lo)
        end = b[TOK - 1 : TOK, :]
        k = k_ref[:, at].astype(F32)
        qd = (q_ref[:, at].astype(F32) * (DK**-0.5) * jnp.exp(b)).astype(BF16)
        kp = (k * jnp.exp(-b)).astype(BF16)
        qd_ref[:, at] = qd
        kd_ref[:, at] = (k * jnp.exp(end - b)).astype(BF16)
        bend_ref[:, at] = end
        for j in range(HEADS // parts):
            h = slice(j * DK, (j + 1) * DK)
            p_ref[i * (HEADS // parts) + j] = mm(qd[:, h], kp[:, h], NT).astype(BF16)


def prep(q, k, g):
    hbm = pl.BlockSpec(memory_space=pltpu.HBM)
    return pl.pallas_call(
        prep_kernel,
        in_specs=[hbm, hbm, hbm],
        out_shape=[
            jax.ShapeDtypeStruct((TOK, HEADS * DK), BF16),
            jax.ShapeDtypeStruct((TOK, HEADS * DK), BF16),
            jax.ShapeDtypeStruct((HEADS, TOK, TOK), BF16),
            jax.ShapeDtypeStruct((1, HEADS * DK), F32),
        ],
        scratch_shapes=[pltpu.VMEM((TOK, HEADS * DK), BF16)] * 3
        + [pltpu.SemaphoreType.DMA((4, 3))],
        compiler_params=params(10),
        cost_estimate=cost(2 * 10**9, 4 * 2**20, 2**20),
        name="prep",
    )(q, k, g)


def update_kernel(ex_ref, kd_ref, v_ref, bend_ref, u_ref):
    rows, cols = extra_sums(ex_ref[...])
    w = jnp.exp(cols[TOK - 1 : TOK, :] - cols)
    for h in range(HEADS):
        kd = (kd_ref[:, h * DK : (h + 1) * DK].astype(F32) * w[:, h : h + 1]).astype(BF16)
        u = mm(kd, v_ref[:, h * DV : (h + 1) * DV], TN)
        u_ref[h, 0:DK, :] = u.astype(BF16)
        end = bend_ref[:, h * DK : (h + 1) * DK] + rows[h : h + 1, TOK - 1 : TOK]
        hi = end.astype(BF16)
        lo = (end - hi.astype(F32)).astype(BF16)
        both = jnp.concatenate([hi.astype(F32), lo.astype(F32)], axis=1)
        u_ref[h, DK : DK + EXTRA_ROWS, :] = jnp.broadcast_to(both, (EXTRA_ROWS, DV)).astype(BF16)


def update(ex, kd, v, bend):
    return pl.pallas_call(
        update_kernel,
        out_shape=jax.ShapeDtypeStruct((HEADS, DK + EXTRA_ROWS, DV), BF16),
        compiler_params=params(8),
        cost_estimate=cost(2 * 10**9, 3 * 2**20),
        name="update",
    )(ex, kd, v, bend)


def inside_kernel(ex_ref, p_ref, v_ref, o_ref):
    rows, cols = extra_sums(ex_ref[...])
    keep = lower_ones(TOK)
    for h in range(HEADS):
        gap = jnp.minimum(cols[:, h : h + 1] - rows[h : h + 1, :], 0.0)
        a = jnp.where(keep, p_ref[h].astype(F32) * jnp.exp(gap), 0.0).astype(BF16)
        o_ref[:, h * DV : (h + 1) * DV] = mm(a, v_ref[:, h * DV : (h + 1) * DV]).astype(BF16)


def inside(ex, p, v):
    return pl.pallas_call(
        inside_kernel,
        out_shape=jax.ShapeDtypeStruct((TOK, HEADS * DV), BF16),
        compiler_params=params(10),
        cost_estimate=cost(4 * 10**9, 4 * 2**20, 2**18),
        name="inside",
    )(ex, p, v)


def prefix_kernel(u_ref, s_ref):
    chunks = u_ref.shape[0]
    tail = u_ref[:, DK : DK + EXTRA_ROWS, :].astype(F32)
    ends = tail[:, 0, 0:DK] + tail[:, 0, DK : 2 * DK]
    keep = jnp.transpose(jnp.exp(ends))
    state = jnp.zeros((DK, DV), F32)
    for m in range(chunks):
        s_ref[m] = state.astype(BF16)
        if m + 1 < chunks:
            state = state * keep[:, m : m + 1] + u_ref[m, 0:DK, :].astype(F32)


def prefix(u):
    return pl.pallas_call(
        prefix_kernel,
        out_shape=jax.ShapeDtypeStruct((u.shape[0], DK, DV), BF16),
        compiler_params=params(8),
        cost_estimate=cost(10**8, 2 * 2**20),
        name="prefix",
    )(u)


def heads_kernel(ex_ref, qd_ref, s_ref, o_ref, gain_ref, out_ref):
    _, cols = extra_sums(ex_ref[...])
    grow = jnp.exp(cols)
    for h in range(HEADS):
        at = slice(h * DV, (h + 1) * DV)
        cross = mm(qd_ref[:, h * DK : (h + 1) * DK], s_ref[h])
        o = o_ref[:, at].astype(F32) + cross * grow[:, h : h + 1]
        ms = jnp.mean(o * o, axis=1, keepdims=True)
        out_ref[:, at] = (o * lax.rsqrt(ms + EPS) * gain_ref[:, at]).astype(BF16)


def heads(ex, qd, s, o, gain):
    return pl.pallas_call(
        heads_kernel,
        out_shape=jax.ShapeDtypeStruct((TOK, HEADS * DV), BF16),
        compiler_params=params(10),
        cost_estimate=cost(2 * 10**9, 5 * 2**20),
        name="heads",
    )(ex, qd, s, o, gain)


KB = 1024
EARLY = 17


def early_kernel(x_ref, y_ref, *refs):
    n = len(refs) - 3
    w_hbm, out_ref, w_ref, sems = refs[:n], refs[n], refs[n + 1], refs[n + 2]
    steps = x_ref.shape[1] // KB

    def move(p, i):
        at = slice(i * KB, (i + 1) * KB)
        return pltpu.make_async_copy(w_hbm[p].at[at, :], w_ref.at[p, at, :], sems.at[p, i])

    for p in range(n):
        for i in range(steps):
            move(p, i).start()
    for p in range(n):
        acc = None
        for i in range(steps):
            at = slice(i * KB, (i + 1) * KB)
            move(p, i).wait()
            x = jnp.concatenate([x_ref[:, at], y_ref[:, at]], axis=0)
            part = mm(x, w_ref[p, at, :])
            acc = part if acc is None else acc + part
        out_ref[p] = acc.astype(BF16)


def early(x, y, ws):
    n = len(ws)
    depth, wide = ws[0].shape
    vmem = pl.BlockSpec(memory_space=pltpu.VMEM)
    return pl.pallas_call(
        early_kernel,
        in_specs=[vmem] * 2 + [pl.BlockSpec(memory_space=pltpu.HBM)] * n,
        out_shape=jax.ShapeDtypeStruct((n, 2 * TOK, wide), BF16),
        scratch_shapes=[
            pltpu.VMEM((n, depth, wide), BF16),
            pltpu.SemaphoreType.DMA((n, depth // KB)),
        ],
        compiler_params=params(EARLY),
        cost_estimate=cost(4 * TOK * depth * wide * n, 2 * depth * wide * n),
    )(x, y, *ws)


PITCH = 24
ROW = 16


def route_kernel(
    place_ref,
    slot_ref,
    e_ref,
    l_ref,
    es_ref,
    ls_ref,
    skip_ref,
    g1_ref,
    g2_ref,
    res_ref,
    out_ref,
    proj_ref,
    row_ref,
):
    out_ref[...] = jnp.zeros_like(out_ref)
    n = 0
    for ref in (e_ref, l_ref, es_ref, ls_ref):
        for p in range(ref.shape[0]):
            proj_ref[place_ref[n]] = ref[p, 0:TOK, :].astype(F32)
            n += 1
    wide = proj_ref.shape[2]
    ms = jnp.zeros((TOK, 1), F32)
    for d in range(n):
        pr = proj_ref[d]
        ms += jnp.sum(pr * pr, axis=1, keepdims=True)
    inv = lax.rsqrt(ms * (1.0 / D) + EPS)
    ms = jnp.zeros((TOK, 1), F32)
    for d in range(n):
        at = slice(d * wide, (d + 1) * wide)
        r = (skip_ref[:, at].astype(F32) + proj_ref[d] * inv * g1_ref[:, at]).astype(BF16)
        res_ref[:, at] = r
        rf = r.astype(F32)
        proj_ref[d] = rf
        ms += jnp.sum(rf * rf, axis=1, keepdims=True)
    inv = lax.rsqrt(ms * (1.0 / D) + EPS)
    for d in range(n):
        at = slice(d * wide, (d + 1) * wide)
        ein = proj_ref[d] * inv * g2_ref[:, at]
        for j in range(wide // 128):
            row_ref[pl.ds(d * (wide // 128) + j, TOK, stride=PITCH), :] = ein[
                :, j * 128 : (j + 1) * 128
            ]

    def body(t, _):
        row = row_ref[pl.ds(pl.multiple_of(t * PITCH, 8), ROW), :].astype(BF16)
        out_ref[slot_ref[TOP * t]] = row
        out_ref[slot_ref[TOP * t + 1]] = row
        return 0

    lax.fori_loop(0, TOK, body, 0, unroll=8)


def route(place, slots, e, l, es, ls, skip, g1, g2, rows):
    wide = e.shape[2]
    vmem = pl.BlockSpec(memory_space=pltpu.VMEM)
    return pl.pallas_call(
        route_kernel,
        in_specs=[pl.BlockSpec(memory_space=pltpu.SMEM)] * 2 + [vmem] * 7,
        out_shape=[
            jax.ShapeDtypeStruct((TOK, D), BF16),
            jax.ShapeDtypeStruct((rows, ROW, 128), BF16),
        ],
        scratch_shapes=[
            pltpu.VMEM((D // wide, TOK, wide), F32),
            pltpu.VMEM((TOK * PITCH, 128), F32),
        ],
        compiler_params=params(12),
        cost_estimate=cost(10**8, 3 * 2**20),
        name="route",
    )(place, slots, e, l, es, ls, skip, g1, g2)


def expert_kernel(x_ref, wg_hbm, wu_hbm, wd_hbm, out_ref, wg_ref, wu_ref, wd_ref, hid_ref, sems):
    parts = 4
    fb = FF // parts

    def moves(i):
        at = slice(i * fb, (i + 1) * fb)
        return (
            pltpu.make_async_copy(wg_hbm.at[:, at], wg_ref.at[:, at], sems.at[0, i]),
            pltpu.make_async_copy(wu_hbm.at[:, at], wu_ref.at[:, at], sems.at[1, i]),
            pltpu.make_async_copy(wd_hbm.at[at, :], wd_ref.at[at, :], sems.at[2, i]),
        )

    for n in range(2):
        for i in range(parts):
            for m in moves(i)[0:2] if n == 0 else moves(i)[2:]:
                m.start()
    x = x_ref[...]
    for i in range(parts):
        at = slice(i * fb, (i + 1) * fb)
        for m in moves(i)[0:2]:
            m.wait()
        gate = mm(x, wg_ref[:, at])
        up = mm(x, wu_ref[:, at])
        hid_ref[:, at] = (gate * jax.nn.sigmoid(gate) * up).astype(BF16)
    for i in range(parts):
        moves(i)[2].wait()
    hid = hid_ref[...]
    nb = 512
    for i in range(D // nb):
        at = slice(i * nb, (i + 1) * nb)
        out_ref[:, at] = mm(hid, wd_ref[:, at]).astype(BF16)


def experts(x, wg, wu, wd):
    rows = x.shape[0]
    hbm = pl.BlockSpec(memory_space=pltpu.HBM)
    return pl.pallas_call(
        expert_kernel,
        in_specs=[pl.BlockSpec(memory_space=pltpu.VMEM), hbm, hbm, hbm],
        out_shape=jax.ShapeDtypeStruct((rows, D), BF16),
        scratch_shapes=[
            pltpu.VMEM((D, FF), BF16),
            pltpu.VMEM((D, FF), BF16),
            pltpu.VMEM((FF, D), BF16),
            pltpu.VMEM((rows, FF), BF16),
            pltpu.SemaphoreType.DMA((3, 4)),
        ],
        compiler_params=params(48),
        cost_estimate=cost(6 * rows * D * FF, 6 * D * FF),
        name="experts",
    )(x, wg, wu, wd)


def combine_kernel(slot_ref, w_ref, back_ref, res_ref, gain_ref, out_ref, row_ref, sq_ref):
    def body(i, _):
        for j in range(8):
            t = i * 8 + j
            a = back_ref[slot_ref[TOP * t]].astype(F32) * w_ref[TOP * t]
            b = back_ref[slot_ref[TOP * t + 1]].astype(F32) * w_ref[TOP * t + 1]
            c = a + b
            row_ref[pl.ds(pl.multiple_of(t * PITCH, 8), ROW), :] = c
            sq_ref[pl.ds(t, 1), :] = jnp.sum(c * c, axis=0, keepdims=True)
        return 0

    lax.fori_loop(0, TOK // 8, body, 0)
    ms = jnp.sum(sq_ref[...], axis=1, keepdims=True) * (1.0 / D)
    inv = lax.rsqrt(ms + EPS)
    for j in range(ROW):
        at = slice(j * 128, (j + 1) * 128)
        c = row_ref[pl.ds(j, TOK, stride=PITCH), :]
        out_ref[:, at] = (res_ref[:, at].astype(F32) + c * inv * gain_ref[:, at]).astype(BF16)


def combine(slots, weights, back, res, gain):
    smem = pl.BlockSpec(memory_space=pltpu.SMEM)
    vmem = pl.BlockSpec(memory_space=pltpu.VMEM)
    return pl.pallas_call(
        combine_kernel,
        in_specs=[smem, smem, vmem, vmem, vmem],
        out_shape=jax.ShapeDtypeStruct((TOK, D), BF16),
        scratch_shapes=[pltpu.VMEM((TOK * PITCH, 128), F32), pltpu.VMEM((TOK, 128), F32)],
        compiler_params=params(8),
        cost_estimate=cost(10**7, 3 * 2**20),
        name="combine",
    )(slots, weights, back, res, gain)


def layer(
    skip_stream_entering,
    mapped_probe_matrix,
    mapped_lookup_matrix,
    mapped_content_matrix,
    retention_preactivation,
    extra_shrinkage,
    attention_group_scale,
    final_projection_matrix,
    blender_branch_scale,
    specialist_prenormal_scale,
    specialist_switch_matrix,
    specialist_expand_matrix,
    specialist_contract_matrix,
    specialist_branch_scale,
    assigned_specialists,
    dispatcher_logits,
):
    sp_count = lax.axis_size("sp")
    dp_count = lax.axis_size("dp")
    total = sp_count * dp_count

    core = lax.axis_index("dp") % 2
    ychip = lax.axis_index("dp") // 2
    ychips = dp_count // 2

    def ring(sign):
        out = []
        for d in range(dp_count):
            y, c = d // 2, d % 2
            s = sign if c == 0 else -sign
            out.append((d, ((y + s) % ychips) * 2 + c))
        return out

    swap = [(d, d ^ 1) for d in range(dp_count)]
    w_own = final_projection_matrix
    w_a = lax.ppermute(w_own, "dp", ring(1))
    w_b = lax.ppermute(w_own, "dp", ring(-1))

    q = mapped_probe_matrix[0]
    k = mapped_lookup_matrix[0]
    v = mapped_content_matrix[0]
    g = retention_preactivation[0]
    ex = lax.all_to_all(
        extra_shrinkage[0].reshape(sp_count, 1, TOK),
        "sp",
        split_axis=0,
        concat_axis=0,
        tiled=True,
    ).reshape(HEADS, TOK)
    qd, kd, p, bend = prep(q, k, g)
    u = update(ex, kd, v, bend)
    u_in = lax.all_to_all(u, "sp", split_axis=0, concat_axis=0, tiled=True)
    s = prefix(u_in)
    s_in = lax.all_to_all(s, "sp", split_axis=0, concat_axis=0, tiled=True)
    o_in = inside(ex, p, v)
    w_a2 = lax.ppermute(w_a, "dp", ring(1))

    head_out = heads(ex, qd, s_in, o_in, attention_group_scale.reshape(1, HEADS * DV))
    head_other = lax.ppermute(head_out, "dp", swap)

    sgn = 1 - 2 * core
    other = 1 - core
    y_up = (ychip + sgn) % ychips
    y_down = (ychip - sgn) % ychips
    y_far = (ychip + 2) % ychips
    place = jnp.stack(
        [
            ychip * 2 + core,
            y_down * 2 + core,
            y_up * 2 + core,
            y_far * 2 + core,
            ychip * 2 + other,
            y_up * 2 + other,
            y_down * 2 + other,
            y_far * 2 + other,
        ]
    ).astype(jnp.int32)
    e = early(head_out, head_other, [w_own, w_a, w_b])
    es = lax.ppermute(e[:, TOK:], "dp", swap)
    l = early(head_out, head_other, [w_a2])
    ls = lax.ppermute(l[:, TOK:], "dp", swap)
    chosen = assigned_specialists[0].reshape(-1)
    onehot = (chosen[:, None] == jnp.arange(total, dtype=jnp.int32)[None, :]).astype(jnp.int32)
    ranks = jnp.sum((jnp.cumsum(onehot, axis=0) - onehot) * onehot, axis=1)
    slots = chosen * CAP + ranks
    weights = dispatcher_logits[0]
    weights = (weights / jnp.sum(weights, axis=1, keepdims=True)).reshape(-1)

    residual, outgoing = route(
        place,
        slots,
        e,
        l,
        es,
        ls,
        skip_stream_entering[0],
        blender_branch_scale.reshape(1, D),
        specialist_prenormal_scale.reshape(1, D),
        total * CAP,
    )
    arrived = lax.all_to_all(
        outgoing.reshape(total, CAP, ROW, 128),
        ("sp", "dp"),
        split_axis=0,
        concat_axis=0,
        tiled=True,
    )
    result = experts(
        arrived.reshape(total * CAP, D),
        specialist_switch_matrix[0],
        specialist_expand_matrix[0],
        specialist_contract_matrix[0],
    )
    back = lax.all_to_all(
        result.reshape(total, CAP, ROW, 128),
        ("sp", "dp"),
        split_axis=0,
        concat_axis=0,
        tiled=True,
    ).reshape(total * CAP, ROW, 128)
    out = combine(slots, weights, back, residual, specialist_branch_scale.reshape(1, D))
    return out.reshape(1, TOK, D)


def solution(mesh):
    return jax.shard_map(
        layer,
        mesh=mesh,
        in_specs=(
            P("dp", "sp", None),
            P("dp", "sp", None),
            P("dp", "sp", None),
            P("dp", "sp", None),
            P("dp", "sp", None),
            P("dp", "sp", None),
            P(),
            P(None, "dp"),
            P(),
            P(),
            P(("sp", "dp"), None, None),
            P(("sp", "dp"), None, None),
            P(("sp", "dp"), None, None),
            P(),
            P("dp", "sp", None),
            P("dp", "sp", None),
        ),
        out_specs=P("dp", "sp", None),
        check_vma=False,
    )
```

time: 195 us -> 185 us (0.949)
  blocking collectives: 29.4 us -> 57.9 us
  waiting for transfers between devices: 78 us -> 60.2 us
  Pallas kernels: 35.9 us -> 27.7 us
  starting transfers between devices: 35.7 us -> 27.9 us
  local copies, waits for them, and re-layouts: 14.7 us -> 9.83 us
    all_to_all x1 -> x2, blocking collectives: 29.4 us -> 57.9 us  [the longest x1 34.1 us: layer(): lax.all_to_all(outgoing.reshape(total, CAP, ROW, 128), ('sp', 'dp'), spli...]
    all_to_all x4 -> x3, waiting for transfers between devices: 54.1 us -> 34.9 us  [the longest x1 24 us: layer(): lax.all_to_all(result.reshape(total, CAP, ROW, 128), ('sp', 'dp'), split_...]
    all_to_all x4 -> x3, starting transfers between devices: 26 us -> 16.2 us  [the longest x1 7.6 us: layer(): lax.all_to_all(extra_shrinkage[0].reshape(sp_count, 1, TOK), 'sp', split_...]
    pallas_call x5, Pallas kernels: 26.7 us -> 20.3 us  [the longest x2 8.11 us: early(): pl.pallas_call(early_kernel, in_specs=[vmem] * 2 + [pl.BlockSpec(memory_s...]
    unnamed x43 -> x35, local copies, waits for them, and re-layouts: 12.8 us -> 8.27 us
    ppermute x7 -> x6, starting transfers between devices: 9.77 us -> 11.7 us  [the longest x1 3.55 us: layer(): w_a = lax.ppermute(w_own, 'dp', ring(1))]
    ppermute x7 -> x6, waiting for transfers between devices: 23.8 us -> 25.3 us  [the longest x1 24.2 us: layer(): w_b = lax.ppermute(w_own, 'dp', ring(-1))]
  transfers between devices with their start and end apart: 11 -> 9, of which waited for: 5 -> 4; matrix products, arithmetic and copies ran while one was open for 1% -> 1% of each run, Pallas kernels for 9% -> 9%
where the time goes in v2:
time: 185 us; the launch traced here: 184 us
  waiting for transfers between devices  60.2 us (33%)
  blocking collectives  57.9 us (31%)
  starting transfers between devices  27.9 us (15%)
  Pallas kernels  27.7 us (15%)
  local copies, waits for them, and re-layouts  9.83 us (5%)
    all_to_all x1, blocking collectives, layer(): lax.all_to_all(outgoing.reshape(total, CAP, ROW, 128), ('sp', 'dp'), spli...  34.1 us
    ppermute x1, waiting for transfers between devices, layer(): w_b = lax.ppermute(w_own, 'dp', ring(-1))  24.2 us
    all_to_all x1, waiting for transfers between devices, layer(): lax.all_to_all(result.reshape(total, CAP, ROW, 128), ('sp', 'dp'), split_...  24 us
    all_to_all x1, blocking collectives, layer(): u_in = lax.all_to_all(u, 'sp', split_axis=0, concat_axis=0, tiled=True)  23.8 us
    all_to_all x1, waiting for transfers between devices, layer(): s_in = lax.all_to_all(s, 'sp', split_axis=0, concat_axis=0, tiled=True)  10.9 us
    unnamed x35, local copies, waits for them, and re-layouts  8.27 us
    pallas_call x2, Pallas kernels, early(): pl.pallas_call(early_kernel, in_specs=[vmem] * 2 + [pl.BlockSpec(memory_s...  8.11 us
    all_to_all x1, starting transfers between devices, layer(): lax.all_to_all(extra_shrinkage[0].reshape(sp_count, 1, TOK), 'sp', split_...  7.6 us
  transfers between devices with their start and end apart: 9, of which 4 were waited for; matrix products, arithmetic and copies ran while one was open for 1% of the time, Pallas kernels for 9%

profile of v2, /device:TPU:1, one launch (start us, length us, event | category | flops | bytes accessed | tf_op | source)
XLA Modules:
  0.0 184.3 jit_solution(4640396361825549127)
XLA Ops:
  0.0 3.6 %collective-permute-start.1 = (bf16[4096,256]{1,0:T(8,128)(2,1)}, bf16[4096,256]{1,0:T(8,128)(2,1)}, u32[]{:S(2)}, u32[]{:S(2)}) collective-permute-start(bf16[4096,256]{1,0:T(8,128)(2,1)} %refs_0_.1), channel_id=1, source_target_pairs={{0,2},{1,7},{2,4},{3,1},{4,6},{5,3},{6,0},{7,5},{8,10},{9,15},{10,... | collective-permute-start | bytes 6291464 | tf_op jit(solution)/shard_map/ppermute | solution.py:447
  3.6 7.6 %all-to-all-start = ((f32[16,1,128]{2,1,0:T(1,128)}), f32[16,1,128]{2,1,0:T(1,128)S(1)}, u32[]{:S(2)}, u32[]{:S(2)}) async-start(f32[16,1,128]{2,1,0:T(1,128)} %bitcast.68), calls=%async_computation | async-start | bytes 16384 | tf_op jit(solution)/shard_map/all_to_all | solution.py:454
  14.3 2.9 %prep.1 = (bf16[128,2048]{1,0:T(8,128)(2,1)S(1)}, bf16[128,2048]{1,0:T(8,128)(2,1)S(1)}, bf16[16,128,128]{2,1,0:T(8,128)(2,1)S(1)}, f32[1,2048]{1,0:T(1,128)S(1)}) custom-call(bf16[128,2048]{1,0:T(8,128)(2,1)S(1)} %bitcast.59, bf16[128,2048]{1,0:T(8,128)(2,1)S(1)} %bitcast.60, bf16[128,2048]{1,0:T(8,128)(2,1)S(1)} %bitcast.61), custom_call_target="tpu_custom_call" | custom-call | flops 2000000000 | bytes 4194304 | tf_op jit(solution)/shard_map/prep/pallas_call | solution.py:100
  18.0 1.1 update.1
  19.1 23.8 %all_to_all.25.u_ref = bf16[16,136,256]{2,1,0:T(8,128)(2,1)S(1)} all-to-all(bf16[16,136,256]{2,1,0:T(8,128)(2,1)S(1)} %update.1), channel_id=1, replica_groups=mesh['sp'=16,'dp'=8] {'sp'}, dimensions={0} | all-to-all | bytes 2228224 | tf_op jit(solution)/shard_map/all_to_all | solution.py:463
  42.9 1.5 prefix.1
  44.4 3.7 %all-to-all-start.2 = ((bf16[16,128,256]{2,1,0:T(8,128)(2,1)}), bf16[16,128,256]{2,1,0:T(8,128)(2,1)S(1)}, u32[]{:S(2)}, u32[]{:S(2)}) async-start(bf16[16,128,256]{2,1,0:T(8,128)(2,1)} %prefix.1), calls=%async_computation.2 | async-start | bytes 2097152 | tf_op jit(solution)/shard_map/all_to_all | solution.py:465
  48.1 2.7 %collective-permute-start.3 = (bf16[4096,256]{1,0:T(8,128)(2,1)}, bf16[4096,256]{1,0:T(8,128)(2,1)}, u32[]{:S(2)}, u32[]{:S(2)}) collective-permute-start(bf16[4096,256]{1,0:T(8,128)(2,1)} %collective-permute-done.1.refs_1_), channel_id=1, source_target_pairs={{0,2},{1,7},{2,4},{3,1},{4,6},{5,3},{6,0},{7,5},{8,10},{9,15},{10,... | collective-permute-start | bytes 6291464 | tf_op jit(solution)/shard_map/ppermute | solution.py:467
  52.6 10.9 %all-to-all-done.2.s_ref = bf16[16,128,256]{2,1,0:T(8,128)(2,1)S(1)} async-done(((bf16[16,128,256]{2,1,0:T(8,128)(2,1)}), bf16[16,128,256]{2,1,0:T(8,128)(2,1)S(1)}, u32[]{:S(2)}, u32[]{:S(2)}) %all-to-all-start.2) | async-done | bytes 1048608 | tf_op jit(solution)/shard_map/all_to_all | solution.py:465
  63.5 1.0 copy-done.10
  64.5 1.7 heads.1.x_ref
  66.3 3.1 %collective-permute-start = (bf16[128,4096]{1,0:T(8,128)(2,1)S(1)}, bf16[128,4096]{1,0:T(8,128)(2,1)S(1)}, u32[]{:S(2)}, u32[]{:S(2)}) collective-permute-start(bf16[128,4096]{1,0:T(8,128)(2,1)S(1)} %heads.1.x_ref), channel_id=1, source_target_pairs={{0,1},{1,0},{2,3},{3,2},{4,5},{5,4},{6,7},{7,6},{8,9},{9,8},{10,11... | collective-permute-start | bytes 3145736 | tf_op jit(solution)/shard_map/ppermute | solution.py:470
  70.3 24.2 %collective-permute-done.2.refs_2_ = bf16[4096,256]{1,0:T(8,128)(2,1)} collective-permute-done((bf16[4096,256]{1,0:T(8,128)(2,1)}, bf16[4096,256]{1,0:T(8,128)(2,1)}, u32[]{:S(2)}, u32[]{:S(2)}) %collective-permute-start.2) | collective-permute-done | bytes 2097184 | tf_op jit(solution)/shard_map/ppermute | solution.py:448
  94.6 5.5 %shard_map.154.e_ref = bf16[3,256,256]{2,1,0:T(8,128)(2,1)S(1)} custom-call(bf16[128,4096]{1,0:T(8,128)(2,1)S(1)} %heads.1.x_ref, bf16[128,4096]{1,0:T(8,128)(2,1)S(1)} %collective-permute-done.y_ref, bf16[4096,256]{1,0:T(8,128)(2,1)} %refs_0_.1, bf16[4096,256]{1,0:T(8,128)(2,1)} %collective-permute-done.1.refs_1_, ...), custom_call_target="tpu_custom_call" | custom-call | flops 1610612736 | bytes 6291456 | tf_op jit(solution)/shard_map/pallas_call | solution.py:234
  100.7 2.0 %collective-permute-start.4 = (bf16[3,128,256]{2,1,0:T(8,128)(2,1)}, bf16[3,128,256]{2,1,0:T(8,128)(2,1)S(1)}, u32[]{:S(2)}, u32[]{:S(2)}) collective-permute-start(bf16[3,128,256]{2,1,0:T(8,128)(2,1)} %slice.17), channel_id=1, source_target_pairs={{0,1},{1,0},{2,3},{3,2},{4,5},{5,4},{6,7},{7,6},{8,9},{9,8},{10,11... | collective-permute-start | bytes 589832 | tf_op jit(solution)/shard_map/ppermute | solution.py:490
  102.7 2.6 %shard_map.155.l_ref = bf16[1,256,256]{2,1,0:T(8,128)(2,1)S(1)} custom-call(bf16[128,4096]{1,0:T(8,128)(2,1)S(1)} %heads.1.x_ref, bf16[128,4096]{1,0:T(8,128)(2,1)S(1)} %collective-permute-done.y_ref, bf16[4096,256]{1,0:T(8,128)(2,1)} %collective-permute-done.3.refs_0_), custom_call_target="tpu_custom_call" | custom-call | flops 536870912 | bytes 2097152 | tf_op jit(solution)/shard_map/pallas_call | solution.py:234
  105.8 1.1 collective-permute-done.5.ls_ref
  106.9 1.9 %route.1 = (bf16[128,2048]{1,0:T(8,128)(2,1)S(1)}, bf16[384,16,128]{2,1,0:T(8,128)(2,1)S(1)}) custom-call(s32[8]{0:T(128)S(1)} %stack.35.place_ref, s32[256]{0:T(256)S(1)} %multiply_add_fusion.slot_ref, bf16[3,256,256]{2,1,0:T(8,128)(2,1)S(1)} %shard_map.154.e_ref, bf16[1,256,256]{2,1,0:T(8,128)(2,1)S(1)} %shard_map.155.l_ref, ...), custom_call_target="tpu_custom_call" | custom-call | flops 100000000 | bytes 3145728 | tf_op jit(solution)/shard_map/route/pallas_call | solution.py:307
  108.8 34.1 %all_to_all.26 = bf16[128,3,16,128]{3,2,1,0:T(8,128)(2,1)S(1)} all-to-all(bf16[128,3,16,128]{3,2,1,0:T(8,128)(2,1)S(1)} %bitcast.47), channel_id=1, replica_groups=mesh['sp'=16,'dp'=8] {'sp','dp'}, dimensions={0} | all-to-all | bytes 3145728 | tf_op jit(solution)/shard_map/all_to_all | solution.py:512
  143.3 7.4 %experts.1 = bf16[384,2048]{1,0:T(8,128)(2,1)S(1)} custom-call(bf16[384,2048]{1,0:T(8,128)(2,1)S(1)} %bitcast.48, bf16[2048,1024]{1,0:T(8,128)(2,1)} %bitcast.69, bf16[2048,1024]{1,0:T(8,128)(2,1)} %bitcast.70, bf16[1024,2048]{1,0:T(8,128)(2,1)} %bitcast.71), custom_call_target="tpu_custom_call" | custom-call | flops 4831838208 | bytes 12582912 | tf_op jit(solution)/shard_map/experts/pallas_call | solution.py:360
  150.8 1.6 copy.28
  152.4 5.0 %all-to-all-start.4 = ((bf16[128,3,16,128]{3,2,1,0:T(8,128)(2,1)}), bf16[128,3,16,128]{3,2,1,0:T(8,128)(2,1)S(1)}, u32[]{:S(2)}, u32[]{:S(2)}) async-start(bf16[128,3,16,128]{3,2,1,0:T(8,128)(2,1)} %bitcast.63), calls=%async_computation.4 | async-start | bytes 3145728 | tf_op jit(solution)/shard_map/all_to_all | solution.py:525
  157.9 24.0 %all-to-all-done.4 = bf16[128,3,16,128]{3,2,1,0:T(8,128)(2,1)S(1)} async-done(((bf16[128,3,16,128]{3,2,1,0:T(8,128)(2,1)}), bf16[128,3,16,128]{3,2,1,0:T(8,128)(2,1)S(1)}, u32[]{:S(2)}, u32[]{:S(2)}) %all-to-all-start.4) | async-done | bytes 1572896 | tf_op jit(solution)/shard_map/all_to_all | solution.py:525
  181.9 2.4 %combine.1 = bf16[128,2048]{1,0:T(8,128)(2,1)} custom-call(s32[256]{0:T(256)S(1)} %multiply_add_fusion.slot_ref, f32[256]{0:T(256)S(1)} %div.21.w_ref, bf16[384,16,128]{2,1,0:T(8,128)(2,1)S(1)} %bitcast.46, bf16[128,2048]{1,0:T(8,128)(2,1)S(1)} %get-tuple-element.16.res_ref, f32[1,2048]{1,0:T(1,128)S(1)} %bitcast.53), custom_call_target="tpu_custom_call" | custom-call | flops 10000000 | bytes 3145728 | tf_op jit(solution)/shard_map/combine/pallas_call | solution.py:400
  (60 shorter events, 8.8 us)
Async XLA Ops:
  0.0 48.1 %collective-permute-start.1 = (bf16[4096,256]{1,0:T(8,128)(2,1)}, bf16[4096,256]{1,0:T(8,128)(2,1)}, u32[]{:S(2)}, u32[]{:S(2)}) collective-permute-start(bf16[4096,256]{1,0:T(8,128)(2,1)} %refs_0_.1), channel_id=1, source_target_pairs={{0,2},{1,7},{2,4},{3,1},{4,6},{5,3},{6,0},{7,5},{8,10},{9,15},{10,... | collective-permute-start | bytes 6291464 | tf_op jit(solution)/shard_map/ppermute | solution.py:447
  3.6 14.4 %all-to-all-start = ((f32[16,1,128]{2,1,0:T(1,128)}), f32[16,1,128]{2,1,0:T(1,128)S(1)}, u32[]{:S(2)}, u32[]{:S(2)}) async-start(f32[16,1,128]{2,1,0:T(1,128)} %bitcast.68), calls=%async_computation | async-start | bytes 16384 | tf_op jit(solution)/shard_map/all_to_all | solution.py:454
  11.2 1.0 copy-start.5
  12.2 1.0 copy-start.6
  13.2 1.0 copy-start.7
  14.3 3.7 %copy-start.4 = (bf16[1,128,4096]{2,1,0:T(8,128)(2,1)S(1)}, bf16[1,128,4096]{2,1,0:T(8,128)(2,1)}, u32[]{:S(2)}) copy-start(bf16[1,128,4096]{2,1,0:T(8,128)(2,1)} %param.19) | copy-start | bytes 3145732
  17.2 0.8 copy-start.9
  18.0 1.1 copy-start.11
  44.4 19.1 %all-to-all-start.2 = ((bf16[16,128,256]{2,1,0:T(8,128)(2,1)}), bf16[16,128,256]{2,1,0:T(8,128)(2,1)S(1)}, u32[]{:S(2)}, u32[]{:S(2)}) async-start(bf16[16,128,256]{2,1,0:T(8,128)(2,1)} %prefix.1), calls=%async_computation.2 | async-start | bytes 2097152 | tf_op jit(solution)/shard_map/all_to_all | solution.py:465
  48.0 46.5 %collective-permute-start.2 = (bf16[4096,256]{1,0:T(8,128)(2,1)}, bf16[4096,256]{1,0:T(8,128)(2,1)}, u32[]{:S(2)}, u32[]{:S(2)}) collective-permute-start(bf16[4096,256]{1,0:T(8,128)(2,1)} %refs_0_.1), channel_id=1, source_target_pairs={{0,6},{1,3},{2,0},{3,5},{4,2},{5,7},{6,4},{7,1},{8,14},{9,11},{10,... | collective-permute-start | bytes 6291464 | tf_op jit(solution)/shard_map/ppermute | solution.py:448
  48.1 54.6 %collective-permute-start.3 = (bf16[4096,256]{1,0:T(8,128)(2,1)}, bf16[4096,256]{1,0:T(8,128)(2,1)}, u32[]{:S(2)}, u32[]{:S(2)}) collective-permute-start(bf16[4096,256]{1,0:T(8,128)(2,1)} %collective-permute-done.1.refs_1_), channel_id=1, source_target_pairs={{0,2},{1,7},{2,4},{3,1},{4,6},{5,3},{6,0},{7,5},{8,10},{9,15},{10,... | collective-permute-start | bytes 6291464 | tf_op jit(solution)/shard_map/ppermute | solution.py:467
  50.8 1.0 copy-start.12
  51.8 11.6 %copy-start.8 = (f32[4096]{0:T(1024)S(1)}, f32[4096]{0:T(1024)}, u32[]{:S(2)}) copy-start(f32[4096]{0:T(1024)} %param.22) | copy-start | bytes 49156
  63.5 1.0 copy-start.10
  64.5 4.9 %copy-start.14 = (s32[1,128,2]{1,2,0:T(2,128)S(1)}, s32[1,128,2]{1,2,0:T(2,128)}, u32[]{:S(2)}) copy-start(s32[1,128,2]{1,2,0:T(2,128)} %param.30) | copy-start | bytes 3076
  66.3 28.3 %collective-permute-start = (bf16[128,4096]{1,0:T(8,128)(2,1)S(1)}, bf16[128,4096]{1,0:T(8,128)(2,1)S(1)}, u32[]{:S(2)}, u32[]{:S(2)}) collective-permute-start(bf16[128,4096]{1,0:T(8,128)(2,1)S(1)} %heads.1.x_ref), channel_id=1, source_target_pairs={{0,1},{1,0},{2,3},{3,2},{4,5},{5,4},{6,7},{7,6},{8,9},{9,8},{10,11... | collective-permute-start | bytes 3145736 | tf_op jit(solution)/shard_map/ppermute | solution.py:470
  100.7 6.2 %copy-start = (bf16[1,128,2048]{2,1,0:T(8,128)(2,1)S(1)}, bf16[1,128,2048]{2,1,0:T(8,128)(2,1)}, u32[]{:S(2)}) copy-start(bf16[1,128,2048]{2,1,0:T(8,128)(2,1)} %param.16) | copy-start | bytes 1572868
  100.7 6.2 %copy-start.1 = (f32[2048]{0:T(1024)S(1)}, f32[2048]{0:T(1024)}, u32[]{:S(2)}) copy-start(f32[2048]{0:T(1024)} %param.24) | copy-start | bytes 24580
  100.7 6.2 %copy-start.2 = (f32[2048]{0:T(1024)S(1)}, f32[2048]{0:T(1024)}, u32[]{:S(2)}) copy-start(f32[2048]{0:T(1024)} %param.25) | copy-start | bytes 24580
  100.7 5.1 %collective-permute-start.4 = (bf16[3,128,256]{2,1,0:T(8,128)(2,1)}, bf16[3,128,256]{2,1,0:T(8,128)(2,1)S(1)}, u32[]{:S(2)}, u32[]{:S(2)}) collective-permute-start(bf16[3,128,256]{2,1,0:T(8,128)(2,1)} %slice.17), channel_id=1, source_target_pairs={{0,1},{1,0},{2,3},{3,2},{4,5},{5,4},{6,7},{7,6},{8,9},{9,8},{10,11... | collective-permute-start | bytes 589832 | tf_op jit(solution)/shard_map/ppermute | solution.py:490
  105.4 1.5 collective-permute-start.5
  152.4 5.0 %copy-start.13 = (f32[1,128,2]{1,2,0:T(2,128)S(1)}, f32[1,128,2]{1,2,0:T(2,128)}, u32[]{:S(2)}) copy-start(f32[1,128,2]{1,2,0:T(2,128)} %param.31) | copy-start | bytes 3076
  152.4 29.5 %copy-start.3 = (f32[2048]{0:T(1024)S(1)}, f32[2048]{0:T(1024)}, u32[]{:S(2)}) copy-start(f32[2048]{0:T(1024)} %param.29) | copy-start | bytes 24580
  152.4 29.5 %all-to-all-start.4 = ((bf16[128,3,16,128]{3,2,1,0:T(8,128)(2,1)}), bf16[128,3,16,128]{3,2,1,0:T(8,128)(2,1)S(1)}, u32[]{:S(2)}, u32[]{:S(2)}) async-start(bf16[128,3,16,128]{3,2,1,0:T(8,128)(2,1)} %bitcast.63), calls=%async_computation.4 | async-start | bytes 3145728 | tf_op jit(solution)/shard_map/all_to_all | solution.py:525
